TPU v7x, 32 devices: a whole 2x2x4 slice. The times are simulated.
32 devices in a mesh: sp: 8 (over z, y), tp: 4 (over x, core).
Axes of the slice: x: 2, y: 2, z: 4, core: 2. Of those that a mesh axis runs over, the one named last changes fastest.
Arguments:
- tokens: bfloat16 [8192, 4096], P('sp', 'tp'), may hold values from -16 to 16
- norm_gain: float32 [4096], replicated, may hold values from 0.1 to 1.9
- w_pool_in: bfloat16 [4096, 2048], P('sp', 'tp'), may hold values from -0.09375 to 0.09375
- w_query: bfloat16 [4096, 2048], P('sp', 'tp'), may hold values from -0.09375 to 0.09375
- w_key: bfloat16 [4096, 256], P('sp', 'tp'), may hold values from -0.09375 to 0.09375
- w_value: bfloat16 [4096, 256], P('sp', 'tp'), may hold values from -0.09375 to 0.09375
- pool_map: bfloat16 [4, 512, 512], P('tp'), may hold values from -0.25 to 0.25
- pool_scale: float32 [2048], P('tp'), may hold values from 0.3 to 3
- q_gain: float32 [64], replicated, may hold values from 0.1 to 1.9
- k_gain: float32 [64], replicated, may hold values from 0.1 to 1.9
- sinks: float32 [32], P('tp'), may hold values from 0 to 4
- w_out: bfloat16 [4096, 4096], P('tp', 'sp'), may hold values from -0.09375 to 0.09375
Outputs:
- layer_out: bfloat16 [8192, 4096], P(('sp', 'tp'))
All inputs are finite; a program needn't handle non-finite values.
Results may differ from a plain program's by a relative error of at most 0.012.
Values may be sent and summed in bfloat16 or wider, within the bound.
A program may use at most 128 MiB of HBM per device.

v0:
```python
import functools

import jax
import jax.numpy as jnp
from jax import lax
from jax.experimental import pallas as pl
from jax.experimental.pallas import tpu as pltpu
from jax.sharding import PartitionSpec as P

HEAD_DIM = 64
GROUP = 8
WINDOW = 128
GROUP_WIDTH = 512
Q_HEADS = 32


epsilon = 1e-06


def passed_along(value, axis, steps):
    count = lax.axis_size(axis)
    first, last = (max(0, -steps), min(count, count - steps))
    return lax.ppermute(value, axis, [(source, source + steps) for source in range(first, last)])


def rms_scale(values):
    return values * lax.rsqrt(jnp.mean(values * values, axis=-1, keepdims=True) + epsilon)


def ring_place(device, count):
    return jnp.where(device % 2 == 0, device // 2, count - 1 - device // 2)


def ring_device(place, count):
    place = (place + count) % count
    return jnp.where(place < count // 2, 2 * place, 2 * (count - 1 - place) + 1)


def partners():
    me = lax.axis_index("tp")
    return me, me + 1 - 2 * (me % 2), (me + 2) % 4


def greet(targets):
    barrier = pltpu.get_barrier_semaphore()
    for axis, target in targets:
        pl.semaphore_signal(
            barrier, inc=1, device_id={axis: target}, device_id_type=pl.DeviceIdType.MESH
        )
    pl.semaphore_wait(barrier, len(targets))


def remote(source, target, send_sem, recv_sem, axis, device):
    return pltpu.make_async_remote_copy(
        src_ref=source,
        dst_ref=target,
        send_sem=send_sem,
        recv_sem=recv_sem,
        device_id={axis: device},
        device_id_type=pl.DeviceIdType.MESH,
    )


def ring_neighbours(count):
    place = ring_place(lax.axis_index("sp"), count)
    return ring_device(place + 1, count), ring_device(place - 1, count)


class Ring:
    def __init__(self, count, own_at, block_at, send, recv):
        self.count, self.last = count, count // 2
        self.place = ring_place(lax.axis_index("sp"), count)
        self.targets = ring_neighbours(count)
        self.own_at, self.block_at, self.send, self.recv = own_at, block_at, send, recv
        self.started, self.previous = [], {}

    def owner(self, distance):
        return ring_device(self.place - distance, self.count)

    def begin(self, step):
        current = {}
        for part in range(2):
            for way in range(2):
                if step == self.last and part != way:
                    continue
                owner = self.owner((1 - 2 * way) * (step - 1))
                if step > 1:
                    self.previous[way, part].wait_recv()
                copy = remote(
                    self.own_at(part) if step == 1 else self.block_at(owner, part),
                    self.block_at(owner, part),
                    self.send.at[way, step - 1, part],
                    self.recv.at[way, step - 1, part],
                    "sp",
                    self.targets[way],
                )
                copy.start()
                current[way, part] = copy
        if step == self.last:
            for key, copy in self.previous.items():
                if key[0] != key[1]:
                    copy.wait_recv()
        self.started += list(current.values())
        self.previous = current

    def arrive(self):
        for copy in self.previous.values():
            copy.wait_recv()

    def sent(self):
        for copy in self.started:
            copy.wait_send()

    def finish(self):
        self.arrive()
        self.sent()


TOKEN_CHUNKS = 4


def gather_kernel(
    count,
    tokens,
    weights,
    all_tokens,
    all_weights,
    own_sem,
    ring_send,
    ring_recv,
    near_send,
    near_recv,
    far_send,
    far_recv,
    pass_send,
    pass_recv,
):
    right, left = ring_neighbours(count)
    me, partner, other = partners()
    rows, width = tokens.shape
    depth = weights.shape[0]
    half = depth // 2
    piece = rows // TOKEN_CHUNKS
    greet([("sp", right), ("sp", left), ("tp", partner), ("tp", other)])

    def token_at(chunk, owner):
        return all_tokens.at[
            pl.ds(chunk * piece, piece), pl.ds(pl.multiple_of(owner * width, width), width)
        ]

    def weight_at(owner, part):
        return all_weights.at[pl.ds(pl.multiple_of(owner * depth + part * half, half), half)]

    far = []
    for chunk in range(TOKEN_CHUNKS):
        copy = remote(
            tokens.at[pl.ds(chunk * piece, piece)],
            token_at(chunk, me),
            far_send.at[chunk],
            far_recv.at[chunk],
            "tp",
            other,
        )
        copy.start()
        far.append(copy)
    passed = []

    def pass_on(chunk):
        far[chunk].wait_recv()
        copy = remote(
            token_at(chunk, other),
            token_at(chunk, other),
            pass_send.at[chunk],
            pass_recv.at[chunk],
            "tp",
            partner,
        )
        copy.start()
        passed.append(copy)

    ring = Ring(
        count,
        lambda part: weights.at[pl.ds(part * half, half)],
        weight_at,
        ring_send,
        ring_recv,
    )
    for step in range(1, ring.last + 1):
        ring.begin(step)
        if step == 1:
            near = remote(
                tokens,
                all_tokens.at[:, pl.ds(pl.multiple_of(me * width, width), width)],
                near_send,
                near_recv,
                "tp",
                partner,
            )
            near.start()
            own = [
                pltpu.make_async_copy(
                    tokens,
                    all_tokens.at[:, pl.ds(pl.multiple_of(me * width, width), width)],
                    own_sem.at[0],
                ),
                pltpu.make_async_copy(
                    weights,
                    all_weights.at[
                        pl.ds(pl.multiple_of(lax.axis_index("sp") * depth, depth), depth)
                    ],
                    own_sem.at[1],
                ),
            ]
            for copy in own:
                copy.start()
        if len(passed) < TOKEN_CHUNKS:
            pass_on(len(passed))
    while len(passed) < TOKEN_CHUNKS:
        pass_on(len(passed))
    ring.finish()
    for copy in far:
        copy.wait_send()
    near.wait()
    for copy in passed:
        copy.wait()
    for copy in own:
        copy.wait()


def gather(tokens, weights):
    count = lax.axis_size("sp")
    rows, width = tokens.shape
    depth, columns = weights.shape
    dma = pltpu.SemaphoreType.DMA
    return pl.pallas_call(
        functools.partial(gather_kernel, count),
        out_shape=(
            jax.ShapeDtypeStruct((rows, width * lax.axis_size("tp")), tokens.dtype),
            jax.ShapeDtypeStruct((depth * count, columns), weights.dtype),
        ),
        in_specs=[pl.BlockSpec(memory_space=pltpu.VMEM)] * 2,
        out_specs=[pl.BlockSpec(memory_space=pl.ANY)] * 2,
        scratch_shapes=[
            dma((2,)),
            dma((2, count // 2, 2)),
            dma((2, count // 2, 2)),
            dma,
            dma,
            dma((TOKEN_CHUNKS,)),
            dma((TOKEN_CHUNKS,)),
            dma((TOKEN_CHUNKS,)),
            dma((TOKEN_CHUNKS,)),
        ],
        compiler_params=pltpu.CompilerParams(collective_id=0, has_side_effects=True),
        cost_estimate=pl.CostEstimate(
            flops=10**9, bytes_accessed=2 * count * depth * columns, transcendentals=0
        ),
    )(tokens, weights)


def project_kernel(
    count,
    mixed,
    w_head,
    w_tail,
    out,
    tails,
    send_near,
    recv_near,
    send_far,
    recv_far,
    own_terms,
    ring_send,
    ring_recv,
    near_send,
    near_recv,
    far_send,
    far_recv,
):
    me, partner, other = partners()
    across = (partner + 2) % 4
    rows = out.shape[0]
    depth, width = w_tail.shape
    half = depth // 2
    head = w_head.shape[0]
    right, left = ring_neighbours(count)
    greet([("sp", right), ("sp", left), ("tp", partner), ("tp", other)])
    ring = Ring(
        count,
        lambda part: w_tail.at[pl.ds(part * half, half)],
        lambda owner, part: tails.at[owner, pl.ds(part * half, half)],
        ring_send,
        ring_recv,
    )
    ring.begin(1)

    def columns(owner):
        return pl.ds(pl.multiple_of(owner * width, width), width)

    def near_copy(chunk):
        return remote(
            send_near.at[chunk],
            recv_near.at[chunk],
            near_send.at[chunk],
            near_recv.at[chunk],
            "tp",
            partner,
        )

    def far_copy(chunk):
        return remote(
            send_far.at[chunk],
            recv_far.at[chunk],
            far_send.at[chunk],
            far_recv.at[chunk],
            "tp",
            other,
        )

    def first(chunk, owner, tail):
        def term(block):
            held = pl.ds(pl.multiple_of(block * rows, rows), rows)
            total = jnp.dot(
                mixed[held, :head], w_head[:, columns(owner)], preferred_element_type=jnp.float32
            )
            total += jnp.dot(mixed[held, head:], tail[...], preferred_element_type=jnp.float32)
            return total.astype(jnp.bfloat16)

        @pl.loop(0, 2)
        def _(pick):
            send_near[chunk, pick] = term(jnp.where(pick == 0, across, partner))

        near_copy(chunk).start()

        @pl.loop(0, 2)
        def _(pick):
            own_terms[chunk, pick] = term(jnp.where(pick == 0, other, me))

    def second(chunk):
        near_copy(chunk).wait_recv()
        send_far[chunk] = (
            own_terms[chunk, 0].astype(jnp.float32) + recv_near[chunk, 0].astype(jnp.float32)
        ).astype(jnp.bfloat16)
        far_copy(chunk).start()

    owners = [ring.owner(0)]
    first(0, owners[0], w_tail)
    second(0)
    for step in range(1, ring.last + 1):
        if step < ring.last:
            ring.begin(step + 1)
            fresh = [ring.owner(step), ring.owner(-step)]
        else:
            ring.arrive()
            fresh = [ring.owner(step)]
        start = len(owners)
        for extra, owner in enumerate(fresh):
            first(start + extra, owner, tails.at[owner])
        for extra in range(len(fresh)):
            second(start + extra)
        owners += fresh
    for chunk, owner in enumerate(owners):
        far_copy(chunk).wait_recv()
        out[:, columns(owner)] = (
            own_terms[chunk, 1].astype(jnp.float32)
            + recv_near[chunk, 1].astype(jnp.float32)
            + recv_far[chunk].astype(jnp.float32)
        ).astype(jnp.bfloat16)
    ring.sent()
    for chunk in range(count):
        near_copy(chunk).wait_send()
        far_copy(chunk).wait_send()


def project(mixed, w_head, w_tail):
    count = lax.axis_size("sp")
    rows = mixed.shape[0] // 4
    depth, width = w_tail.shape
    dma = pltpu.SemaphoreType.DMA
    return pl.pallas_call(
        functools.partial(project_kernel, count),
        out_shape=jax.ShapeDtypeStruct((rows, count * width), jnp.bfloat16),
        in_specs=[pl.BlockSpec(memory_space=pltpu.VMEM)] * 3,
        out_specs=pl.BlockSpec(memory_space=pltpu.VMEM),
        scratch_shapes=[
            pltpu.VMEM((count, depth, width), jnp.bfloat16),
            pltpu.VMEM((count, 2, rows, width), jnp.bfloat16),
            pltpu.VMEM((count, 2, rows, width), jnp.bfloat16),
            pltpu.VMEM((count, rows, width), jnp.bfloat16),
            pltpu.VMEM((count, rows, width), jnp.bfloat16),
            pltpu.VMEM((count, 2, rows, width), jnp.bfloat16),
            dma((2, count // 2, 2)),
            dma((2, count // 2, 2)),
            dma((count,)),
            dma((count,)),
            dma((count,)),
            dma((count,)),
        ],
        compiler_params=pltpu.CompilerParams(
            collective_id=1, has_side_effects=True, vmem_limit_bytes=60000 * 1024
        ),
        cost_estimate=pl.CostEstimate(
            flops=2 * mixed.size * count * width,
            bytes_accessed=2 * mixed.shape[1] * count * width,
            transcendentals=0,
        ),
    )(mixed, w_head, w_tail)


def local(
    tokens,
    norm_gain,
    w_pool_in,
    w_query,
    w_key,
    w_value,
    pool_map,
    pool_scale,
    q_gain,
    k_gain,
    sinks,
    w_out,
):
    tok_rows = tokens.shape[0]
    local_groups = w_key.shape[1] // HEAD_DIM
    seq_index = lax.axis_index("sp")
    group_first = lax.axis_index("tp") * local_groups
    weights = jnp.concatenate([w_pool_in, w_query, w_key, w_value], axis=1)
    gathered, all_weights = gather(tokens, weights)
    head = w_out.shape[0] // 2
    w_head, gathered = lax.optimization_barrier((w_out[:head], gathered))
    head_columns = lax.all_gather(w_head, "sp", axis=1, tiled=True)
    widened = gathered.astype(jnp.float32)
    normed = (rms_scale(widened) * norm_gain).astype(jnp.bfloat16)
    ext_rows = normed.shape[0]
    pool_end = w_pool_in.shape[1]
    query_end = pool_end + w_query.shape[1]
    key_end = query_end + w_key.shape[1]
    sums = jnp.dot(normed, all_weights, preferred_element_type=jnp.float32).astype(jnp.bfloat16)
    pool_sum, query_sum = sums[:, :pool_end], sums[:, pool_end:query_end]
    key_sum, value_sum = sums[:, query_end:key_end], sums[:, key_end:]
    pool_in = pool_sum.astype(jnp.bfloat16)
    query_rows = lax.optimization_barrier(query_sum.astype(jnp.bfloat16))
    key_rows = lax.optimization_barrier(key_sum.astype(jnp.bfloat16))
    value_rows = value_sum.astype(jnp.bfloat16).reshape(ext_rows, local_groups, HEAD_DIM)
    query_float = query_rows.astype(jnp.float32).reshape(ext_rows, local_groups * GROUP, HEAD_DIM)
    query_normed = (
        (rms_scale(query_float) * q_gain)
        .astype(jnp.bfloat16)
        .reshape(ext_rows, local_groups, GROUP, HEAD_DIM)
    )
    key_float = key_rows.astype(jnp.float32).reshape(ext_rows, local_groups, HEAD_DIM)
    key_normed = (rms_scale(key_float) * k_gain).astype(jnp.bfloat16)
    key_width = local_groups * HEAD_DIM
    pair_tail = jnp.concatenate(
        [
            key_normed[tok_rows - WINDOW :].reshape(WINDOW, key_width),
            value_rows[tok_rows - WINDOW :].reshape(WINDOW, key_width),
        ],
        axis=1,
    )
    earlier_pairs, earlier_pool = passed_along((pair_tail, pool_in[tok_rows - 15 :]), "sp", 1)
    key_span = jnp.concatenate(
        [earlier_pairs[:, :key_width].reshape(WINDOW, local_groups, HEAD_DIM), key_normed], axis=0
    )
    value_span = jnp.concatenate(
        [earlier_pairs[:, key_width:].reshape(WINDOW, local_groups, HEAD_DIM), value_rows], axis=0
    )
    pool_span = jnp.concatenate([earlier_pool, pool_in], axis=0)
    positions = seq_index * tok_rows + jnp.arange(tok_rows, dtype=jnp.int32)
    group_ids = group_first + jnp.arange(local_groups, dtype=jnp.int32)
    spans = jnp.exp2((group_ids + 1).astype(jnp.float32))
    pool_float = pool_span.astype(jnp.float32).reshape(tok_rows + 15, local_groups, GROUP_WIDTH)
    sum_two = pool_float[1:] + pool_float[:-1]
    sum_four = sum_two[2:] + sum_two[:-2]
    sum_eight = sum_four[4:] + sum_four[:-4]
    sum_sixteen = sum_eight[8:] + sum_eight[:-8]
    span_pick = spans[None, :, None]
    running = jnp.where(
        span_pick < 3.0,
        sum_two[14 : 14 + tok_rows],
        jnp.where(
            span_pick < 6.0,
            sum_four[12 : 12 + tok_rows],
            jnp.where(span_pick < 12.0, sum_eight[8 : 8 + tok_rows], sum_sixteen),
        ),
    )
    counts = jnp.minimum(positions.astype(jnp.float32)[:, None] + 1.0, spans[None, :])
    pool_diff = (running / counts[:, :, None] - pool_float[15:]).astype(jnp.bfloat16)
    mapped = jnp.einsum("tlc,lcd->tld", pool_diff, pool_map, preferred_element_type=jnp.float32)
    pool_branch = rms_scale(mapped * pool_scale.reshape(local_groups, GROUP_WIDTH))
    blocks = tok_rows // WINDOW
    query_blocks = query_normed.reshape(blocks, WINDOW, local_groups, GROUP, HEAD_DIM)
    key_pairs = jnp.concatenate(
        [
            key_span[:tok_rows].reshape(blocks, WINDOW, local_groups, HEAD_DIM),
            key_span[WINDOW:].reshape(blocks, WINDOW, local_groups, HEAD_DIM),
        ],
        axis=1,
    )
    value_pairs = jnp.concatenate(
        [
            value_span[:tok_rows].reshape(blocks, WINDOW, local_groups, HEAD_DIM),
            value_span[WINDOW:].reshape(blocks, WINDOW, local_groups, HEAD_DIM),
        ],
        axis=1,
    )
    scores = jnp.einsum(
        "nqlgd,nkld->nlgqk", query_blocks, key_pairs, preferred_element_type=jnp.float32
    ) * HEAD_DIM ** (-0.5)
    query_pos = jnp.arange(WINDOW, dtype=jnp.int32)[:, None] + WINDOW
    key_pos = jnp.arange(2 * WINDOW, dtype=jnp.int32)[None, :]
    distance = query_pos - key_pos
    in_band = (distance >= 0) & (distance < WINDOW)
    key_global = (
        seq_index * tok_rows
        + jnp.arange(blocks, dtype=jnp.int32)[:, None] * WINDOW
        - WINDOW
        + jnp.arange(2 * WINDOW, dtype=jnp.int32)[None, :]
    )
    allowed = in_band[None] & (key_global >= 0)[:, None, :]
    head_ids = group_ids[:, None] * GROUP + jnp.arange(GROUP, dtype=jnp.int32)[None, :] + 1
    slopes = jnp.exp2(-8.0 * head_ids.astype(jnp.float32) / Q_HEADS)
    logits = (
        scores - slopes[None, :, :, None, None] * distance.astype(jnp.float32)[None, None, None]
    )
    exp_scores = jnp.exp(jnp.where(allowed[:, None, None], logits, -jnp.inf))
    sink_logits = sinks.reshape(local_groups, GROUP)
    denominator = jnp.sum(exp_scores, axis=-1) + jnp.exp(sink_logits)[None, :, :, None]
    weights_bf = (exp_scores / denominator[..., None]).astype(jnp.bfloat16)
    attended = jnp.einsum(
        "nlgqk,nkld->nqlgd", weights_bf, value_pairs, preferred_element_type=jnp.float32
    )
    attn_branch = rms_scale(attended.reshape(tok_rows, local_groups, GROUP_WIDTH))
    mixed_rows = (
        jnp.stack([pool_branch, attn_branch], axis=2)
        .reshape(tok_rows, 2 * local_groups * GROUP_WIDTH)
        .astype(jnp.bfloat16)
    )
    return project(mixed_rows, head_columns, w_out[head:])


def solution(mesh):
    in_specs = (
        P("sp", "tp"),
        P(),
        P("sp", "tp"),
        P("sp", "tp"),
        P("sp", "tp"),
        P("sp", "tp"),
        P("tp", None, None),
        P("tp"),
        P(),
        P(),
        P("tp"),
        P("tp", "sp"),
    )
    out_specs = P(("sp", "tp"), None)
    return jax.shard_map(local, mesh=mesh, in_specs=in_specs, out_specs=out_specs, check_vma=False)
```

profile of v0, /device:TPU:1, one launch (start us, length us, event | category | flops | bytes accessed | tf_op | source)
XLA Modules:
  0.0 286.9 jit_solution(1031097184839382574)
XLA Ops:
  8.6 2.3 fusion.45
  10.9 1.9 concatenate.21.weights
  12.8 95.7 %shard_map.118 = (bf16[1024,4096]{1,0:T(8,128)(2,1)}, bf16[4096,1152]{1,0:T(8,128)(2,1)}) custom-call(bf16[1024,1024]{1,0:T(8,128)(2,1)} %tokens.1, bf16[512,1152]{1,0:T(8,128)(2,1)} %concatenate.21.weights), custom_call_target="tpu_custom_call" | custom-call | flops 1000000000 | bytes 9437184 | tf_op jit(solution)/shard_map/pallas_call | solution.py:235
  108.5 5.2 %fusion = f32[1024]{0:T(1024)S(1)} fusion(bf16[1024,4096]{1,0:T(8,128)(2,1)} %get-tuple-element.10), kind=kLoop, calls=%fused_computation.2 | loop fusion | flops 12581888 | bytes 8392704 | tf_op jit(solution)/shard_map/reduce_sum | solution.py:27
  114.3 15.2 %fusion.12 = bf16[1024,1152]{1,0:T(8,128)(2,1)S(1)} fusion(bf16[4096,1152]{1,0:T(8,128)(2,1)} %get-tuple-element.11, bf16[1024,4096]{1,0:T(8,128)(2,1)S(1)} %copy-done.2, f32[4096]{0:T(1024)S(1)} %copy-done.16, f32[1024]{0:T(1024)S(1)} %add_rsqrt_fusion.2), kind=kOutput, calls=%fused_computation.15 | convolution fusion | flops 9681633280 | bytes 20205568 | tf_op jit(solution)/shard_map/dot_general | solution.py:439
  130.1 2.7 collective-permute-start
  134.9 4.2 %collective-permute-start.1 = (bf16[128,128]{1,0:T(8,128)(2,1)}, bf16[128,128]{1,0:T(8,128)(2,1)}, u32[]{:S(2)}, u32[]{:S(2)}) collective-permute-start(bf16[128,128]{1,0:T(8,128)(2,1)} %pad_maximum_fusion.3), channel_id=1, source_target_pairs={{0,4},{4,8},{8,12},{12,16},{16,20},{20,24},{24,28},{1,5},{5,9},{9,... | collective-permute-start | bytes 98312 | tf_op jit(solution)/shard_map/ppermute | solution.py:23
  139.1 2.6 fusion.44
  141.8 1.6 convert_multiply_fusion.4
  143.4 1.6 copy.29
  145.7 2.0 copy.30
  150.0 1.1 broadcast_multiply_fusion
  151.1 2.0 multiply_convert_fusion.1
  155.2 1.1 copy.26
  158.6 1.4 multiply_reduce_fusion.1
  160.1 1.3 fusion.23
  162.7 3.5 %fusion.9 = (f32[8,8,128]{2,1,0:T(8,128)S(1)}, f32[8,256,128,8]{2,1,3,0:T(8,128)S(1)}) fusion(f32[8,128,256]{1,2,0:T(8,128)S(1)} %copy-done.7, pred[8,128,256]{1,2,0:T(8,128)(4,1)S(1)} %copy-done.11, bf16[8,128,8,64]{1,0,3,2:T(8,128)(2,1)S(1)} %copy-done.8, bf16[8,128,1,64]{1,3,0,2:T(8,128)(2,1)} %copy.28, bf16[8,128,1,64]{1,3,0,2:T(8,128)(2,1)S(1)} %copy.27), kind=kOutput, calls=%fused_computation.12 | convolution fusion | flops 277340160 | bytes 11042816 | tf_op jit(solution)/shard_map/nqlgd,nkld->nlgqk/dot_general | solution.py:508
  166.3 2.4 multiply_reduce_fusion
  168.7 2.5 copy.34
  171.2 1.9 reshape.363
  174.6 2.6 copy.39.mixed
  177.2 35.7 %all-gather.2.cloned.1.call-done.w_head = bf16[512,4096]{1,0:T(8,128)(2,1)} async-done(((bf16[512,512]{1,0:T(8,128)(2,1)}), bf16[512,4096]{1,0:T(8,128)(2,1)}) %all-gather.2.cloned.1.call-update) | async-done | bytes 4194320 | tf_op jit(solution)/shard_map/all_gather | solution.py:432
  212.9 64.0 %shard_map.119 = bf16[256,4096]{1,0:T(8,128)(2,1)} custom-call(bf16[1024,1024]{1,0:T(8,128)(2,1)} %copy.39.mixed, bf16[512,4096]{1,0:T(8,128)(2,1)} %all-gather.2.cloned.1.call-done.w_head, bf16[512,512]{1,0:T(8,128)(2,1)} %get-tuple-element.18.w_tail), custom_call_target="tpu_custom_call" | custom-call | flops 8589934592 | bytes 8388608 | tf_op jit(solution)/shard_map/pallas_call | solution.py:380
  276.9 3.1 %copy.46 = bf16[256,4096]{1,0:T(8,128)(2,1)} copy(bf16[256,4096]{1,0:T(8,128)(2,1)} %shard_map.119) | data formatting | bytes 4194304
  (79 shorter events, 15.3 us)
Async XLA Ops:
  6.5 151.7 %copy-start = (bf16[1,512,512]{2,1,0:T(8,128)(2,1)S(1)}, bf16[1,512,512]{2,1,0:T(8,128)(2,1)}, u32[]{:S(2)}) copy-start(bf16[1,512,512]{2,1,0:T(8,128)(2,1)} %param.18) | copy-start | bytes 1572868
  6.5 4.3 %copy-start.9 = (bf16[512,512]{1,0:T(8,128)(2,1)S(1)}, bf16[512,512]{1,0:T(8,128)(2,1)}, u32[]{:S(2)}) copy-start(bf16[512,512]{1,0:T(8,128)(2,1)} %param.14) | copy-start | bytes 1572868
  6.5 4.3 %copy-start.10 = (bf16[512,512]{1,0:T(8,128)(2,1)S(1)}, bf16[512,512]{1,0:T(8,128)(2,1)}, u32[]{:S(2)}) copy-start(bf16[512,512]{1,0:T(8,128)(2,1)} %param.15) | copy-start | bytes 1572868
  6.5 206.3 %all-gather.2.cloned.1.call-start = ((), (), s32[]{:S(2)}) async-start(), calls=%async_computation | async-start | bytes 4718592 | tf_op jit(solution)/shard_map/all_gather | solution.py:432
  12.8 100.9 %copy-start.16 = (f32[4096]{0:T(1024)S(1)}, f32[4096]{0:T(1024)}, u32[]{:S(2)}) copy-start(f32[4096]{0:T(1024)} %param.13) | copy-start | bytes 49156
  108.5 5.8 %copy-start.2 = (bf16[1024,4096]{1,0:T(8,128)(2,1)S(1)}, bf16[1024,4096]{1,0:T(8,128)(2,1)}, u32[]{:S(2)}) copy-start(bf16[1024,4096]{1,0:T(8,128)(2,1)} %get-tuple-element.10) | copy-start | bytes 25165828
  114.3 19.7 %copy-start.13 = (f32[64]{0:T(128)S(1)}, f32[64]{0:T(128)}, u32[]{:S(2)}) copy-start(f32[64]{0:T(128)} %param.21) | copy-start | bytes 772
  129.5 4.2 %copy-start.6 = (bf16[1024,1152]{1,0:T(8,128)(2,1)}, bf16[1024,1152]{1,0:T(8,128)(2,1)S(1)}, u32[]{:S(2)}) copy-start(bf16[1024,1152]{1,0:T(8,128)(2,1)S(1)} %fusion.12) | copy-start | bytes 7077892
  130.1 26.2 %collective-permute-start = (bf16[15,512]{1,0:T(8,128)(2,1)}, bf16[15,512]{1,0:T(8,128)(2,1)}, u32[]{:S(2)}, u32[]{:S(2)}) collective-permute-start(bf16[15,512]{1,0:T(8,128)(2,1)} %slice.112), channel_id=1, source_target_pairs={{0,4},{4,8},{8,12},{12,16},{16,20},{20,24},{24,28},{1,5},{5,9},{9,... | collective-permute-start | bytes 46088 | tf_op jit(solution)/shard_map/ppermute | solution.py:23
  134.9 26.4 %collective-permute-start.1 = (bf16[128,128]{1,0:T(8,128)(2,1)}, bf16[128,128]{1,0:T(8,128)(2,1)}, u32[]{:S(2)}, u32[]{:S(2)}) collective-permute-start(bf16[128,128]{1,0:T(8,128)(2,1)} %pad_maximum_fusion.3), channel_id=1, source_target_pairs={{0,4},{4,8},{8,12},{12,16},{16,20},{20,24},{24,28},{1,5},{5,9},{9,... | collective-permute-start | bytes 98312 | tf_op jit(solution)/shard_map/ppermute | solution.py:23
  147.7 1.7 copy-start.3
  149.4 1.7 copy-start.15
  150.0 3.1 %copy-start.12 = (pred[128,256]{0,1:T(8,128)(4,1)S(1)}, pred[128,256]{0,1:T(8,128)(4,1)}, u32[]{:S(2)}) copy-start(pred[128,256]{0,1:T(8,128)(4,1)} %fusion.39) | copy-start | bytes 98308
  151.1 4.1 %copy-start.17 = (f32[8]{0:T(128)S(1)}, f32[8]{0:T(128)}, u32[]{:S(2)}) copy-start(f32[8]{0:T(128)} %param.22) | copy-start | bytes 100
  153.1 3.2 %copy-start.4 = (bf16[1024,512]{1,0:T(8,128)(2,1)S(1)}, bf16[1024,512]{1,0:T(8,128)(2,1)}, u32[]{:S(2)}) copy-start(bf16[1024,512]{1,0:T(8,128)(2,1)} %get-tuple-element.13) | copy-start | bytes 3145732
  157.9 0.7 copy-start.14
  160.0 2.6 copy-start.7
  160.1 2.6 copy-start.8
  160.1 2.6 copy-start.11
  173.2 1.2 copy-start.5
  212.9 67.1 %copy-start.1 = (bf16[1,512,512]{2,1,0:T(8,128)(2,1)S(1)}, bf16[1,512,512]{2,1,0:T(8,128)(2,1)}, u32[]{:S(2)}) copy-start(bf16[1,512,512]{2,1,0:T(8,128)(2,1)} %param.18) | copy-start | bytes 1572868
Sparse Core Ops, SparseCore 0:
  139.2 73.5 all-gather.1
where the time goes:
time: 289 us; the launch traced here: 287 us
  Pallas kernels  160 us (55%)
  waiting for transfers between devices  35.8 us (12%)
  local copies, waits for them, and re-layouts  31.1 us (11%)
  matrix products  22.6 us (8%)
  other arithmetic  17.1 us (6%)
  between operations  13.8 us (5%)
  starting transfers between devices  6.84 us (2%)
    pallas_call x1, Pallas kernels, gather(): pl.pallas_call(functools.partial(gather_kernel, count), out_shape=(jax.Sh...  95.7 us
    pallas_call x1, Pallas kernels, project(): pl.pallas_call(functools.partial(project_kernel, count), out_shape=jax.Sh...  64 us
    all_gather x1, waiting for transfers between devices, local(): head_columns = lax.all_gather(w_head, 'sp', axis=1, tiled=True)  35.7 us
    dot_general x1, matrix products, local(): jnp.dot(normed, all_weights, preferred_element_type=jnp.float32)  15.2 us
    unnamed x40, local copies, waits for them, and re-layouts  8.32 us
    ppermute x2, starting transfers between devices, passed_along(): lax.ppermute(value, axis, [(source, source + steps) for source in range(f...  6.84 us
  transfers between devices with their start and end apart: 3, of which 1 were waited for; matrix products, arithmetic and copies ran while one was open for 13% of the time, Pallas kernels for 0%

commit v1 on v0

v1 whole, which is shorter than its diff:
```python
import functools

import jax
import jax.numpy as jnp
from jax import lax
from jax.experimental import pallas as pl
from jax.experimental.pallas import tpu as pltpu
from jax.sharding import PartitionSpec as P

HEAD_DIM = 64
GROUP = 8
WINDOW = 128
Q_HEADS = 32
LANES = 128
TOKEN_CHUNKS = 4
HALO_ROWS = 16
MASKED = -1e30

epsilon = 1e-06
bf16, f32 = jnp.bfloat16, jnp.float32


def ring_place(device, count):
    return jnp.where(device % 2 == 0, device // 2, count - 1 - device // 2)


def ring_device(place, count):
    place = (place + count) % count
    return jnp.where(place < count // 2, 2 * place, 2 * (count - 1 - place) + 1)


def partners():
    me = lax.axis_index("tp")
    return me, me + 1 - 2 * (me % 2), (me + 2) % 4


def greet(targets):
    barrier = pltpu.get_barrier_semaphore()
    for axis, target in targets:
        pl.semaphore_signal(
            barrier, inc=1, device_id={axis: target}, device_id_type=pl.DeviceIdType.MESH
        )
    pl.semaphore_wait(barrier, len(targets))


def remote(source, target, send_sem, recv_sem, axis, device):
    return pltpu.make_async_remote_copy(
        src_ref=source,
        dst_ref=target,
        send_sem=send_sem,
        recv_sem=recv_sem,
        device_id={axis: device},
        device_id_type=pl.DeviceIdType.MESH,
    )


def aligned(index, size):
    return pl.ds(pl.multiple_of(index * size, size), size)


def dot(left, right):
    return jnp.dot(left, right, preferred_element_type=f32)


class Ring:
    def __init__(self, count, block_at, send, recv):
        self.count, self.last = count, count // 2
        self.place = ring_place(lax.axis_index("sp"), count)
        self.targets = (
            ring_device(self.place + 1, count),
            ring_device(self.place - 1, count),
        )
        self.block_at, self.send, self.recv = block_at, send, recv
        self.started = []
        self.events = [(step, part) for step in range(1, self.last) for part in range(2)]
        self.events.append((self.last, None))
        self.done = 0

    def owner(self, distance):
        return ring_device(self.place - distance, self.count)

    def copy(self, step, way, part):
        block = self.block_at(self.owner((1 - 2 * way) * (step - 1)), part)
        return remote(
            block,
            block,
            self.send.at[way, step - 1, part],
            self.recv.at[way, step - 1, part],
            "sp",
            self.targets[way],
        )

    def start(self, step, way, part):
        self.copy(step, way, part).start()
        self.started.append((step, way, part))

    def begin(self, part):
        for way in range(2):
            if self.last > 1 or part == way:
                self.start(1, way, part)

    def advance(self):
        step, part = self.events[self.done]
        self.done += 1
        for way in range(2):
            held = way if part is None else part
            self.copy(step, way, held).wait_recv()
            if step < self.last and (step + 1 < self.last or held == way):
                self.start(step + 1, way, held)

    def ready(self, step):
        target = len(self.events) if step == self.last else 2 * step
        while self.done < target:
            self.advance()
        return [self.owner(step)] if step == self.last else [self.owner(step), self.owner(-step)]

    def sent(self):
        for step, way, part in self.started:
            self.copy(step, way, part).wait_send()


def layer_kernel(
    count,
    tokens,
    w_pool_in,
    w_query,
    w_key_t,
    w_value_t,
    pool_map,
    w_out,
    gain,
    params,
    out,
    normed,
    first_weights,
    last_weights,
    acc,
    queries,
    keys_low,
    keys_high,
    values_low,
    values_high,
    pool_span,
    pairs,
    mixed,
    bias,
    band,
    ones_block,
    halo_pairs,
    halo_pool,
    recv_near,
    send_far,
    recv_far,
    local_sem,
    first_send,
    first_recv,
    last_send,
    last_recv,
    near_sem,
    far_sem,
    pass_sem,
    halo_sem,
    sum_near_sem,
    sum_far_sem,
):
    me, partner, other = partners()
    across = (partner + 2) % 4
    seq = lax.axis_index("sp")
    rows, width = tokens.shape
    depth, branch = w_pool_in.shape
    head_columns = w_query.shape[1]
    mid = branch + head_columns
    piece = rows // TOKEN_CHUNKS
    blocks = rows // WINDOW
    out_rows = out.shape[0]
    out_width = w_out.shape[1]
    mix = w_out.shape[0]
    pairs_of_heads = head_columns // LANES

    def first_block(owner, part):
        return first_weights.at[
            pl.ds(pl.multiple_of(owner * depth + part * (depth // 2), depth // 2), depth // 2)
        ]

    def last_block(owner, part):
        return last_weights.at[owner, pl.ds(part * (mix // 2), mix // 2)]

    first_ring = Ring(count, first_block, first_send, first_recv)
    last_ring = Ring(count, last_block, last_send, last_recv)
    following = (seq + 1) % count
    preceding = (seq + count - 1) % count

    def columns(owner):
        return aligned(owner, width)

    own_rows = aligned(seq, depth)
    local = [
        pltpu.make_async_copy(source, target, local_sem.at[index])
        for index, (source, target) in enumerate(
            [
                (w_pool_in, first_weights.at[own_rows, pl.ds(0, branch)]),
                (w_query, first_weights.at[own_rows, pl.ds(branch, head_columns)]),
                (tokens, normed.at[:, columns(me)]),
                (w_out, last_weights.at[seq]),
            ]
        )
    ]
    for copy in local:
        copy.start()
    key_value = jnp.concatenate([w_key_t[...], w_value_t[...]], axis=0).astype(f32)
    first_weights[own_rows, pl.ds(mid, LANES)] = key_value.T.astype(bf16)
    greet(
        [
            ("sp", first_ring.targets[0]),
            ("sp", first_ring.targets[1]),
            ("sp", following),
            ("sp", preceding),
            ("tp", partner),
            ("tp", other),
        ]
    )
    local[0].wait()
    local[1].wait()
    first_ring.begin(0)
    first_ring.begin(1)

    def far_copy(chunk):
        return remote(
            tokens.at[pl.ds(chunk * piece, piece)],
            normed.at[pl.ds(chunk * piece, piece), columns(me)],
            far_sem.at[0, chunk],
            far_sem.at[1, chunk],
            "tp",
            other,
        )

    def near_copy():
        return remote(
            tokens, normed.at[:, columns(me)], near_sem.at[0], near_sem.at[1], "tp", partner
        )

    def pass_copy(chunk):
        held = normed.at[pl.ds(chunk * piece, piece), columns(other)]
        return remote(held, held, pass_sem.at[0, chunk], pass_sem.at[1, chunk], "tp", partner)

    for chunk in range(TOKEN_CHUNKS):
        far_copy(chunk).start()
    near_copy().start()

    span = 2.0 * jnp.exp2(me.astype(f32))
    row = lax.broadcasted_iota(jnp.int32, (WINDOW, 2 * WINDOW), 0)
    column = lax.broadcasted_iota(jnp.int32, (WINDOW, 2 * WINDOW), 1)
    distance = (row + WINDOW - column).astype(f32)
    band[...] = jnp.where((distance >= 0.0) & (distance < span), 1.0, 0.0).astype(bf16)
    allowed = (distance >= 0.0) & (distance < float(WINDOW))
    for pair in range(pairs_of_heads):
        for half in range(2):
            head = (me * GROUP + 2 * pair + half + 1).astype(f32)
            slope = jnp.exp2(jnp.full((WINDOW, 2 * WINDOW), -8.0 / Q_HEADS, f32) * head)
            bias[pl.ds(pair * WINDOW, WINDOW), pl.ds(half * 2 * WINDOW, 2 * WINDOW)] = jnp.where(
                allowed, -slope * distance, MASKED
            )
    block_row = lax.broadcasted_iota(jnp.int32, (2 * LANES, 2 * LANES), 0) // HEAD_DIM
    block_column = lax.broadcasted_iota(jnp.int32, (2 * LANES, 2 * LANES), 1) // HEAD_DIM
    ones_block[...] = jnp.where(block_row == block_column, 1.0, 0.0).astype(bf16)
    pool_span[pl.ds(0, WINDOW)] = jnp.zeros((WINDOW, branch), bf16)

    strip = 32

    def normalise(chunk):
        @pl.loop(0, piece // strip)
        def _(index):
            held = pl.ds(pl.multiple_of(chunk * piece + index * strip, strip), strip)
            values = normed[held].astype(f32)
            scale = lax.rsqrt(jnp.mean(values * values, axis=-1, keepdims=True) + epsilon)
            normed[held] = (values * scale * gain[...]).astype(bf16)

    local[2].wait()
    for chunk in range(TOKEN_CHUNKS):
        far_copy(chunk).wait_recv()
        pass_copy(chunk).start()
        if chunk == 0:
            near_copy().wait()
        first_ring_events = len(first_ring.events)
        if chunk < first_ring_events - 1:
            first_ring.advance()
        pass_copy(chunk).wait()
        normalise(chunk)
    for chunk in range(TOKEN_CHUNKS):
        far_copy(chunk).wait_send()

    tile = rows // 4

    def term_of(index, owner):
        return dot(normed[aligned(index, tile), aligned(owner, depth)], first_weights[aligned(owner, depth), :])

    def multiply(owners, fresh):
        @pl.loop(0, rows // tile)
        def _(index):
            total = term_of(index, owners[0])
            for owner in owners[1:]:
                total += term_of(index, owner)
            held = aligned(index, tile)
            acc[held] = total if fresh else acc[held] + total

    multiply([first_ring.owner(0)], True)
    for step in range(1, first_ring.last):
        owners = first_ring.ready(step)
        if step == first_ring.last - 1:
            local[3].wait()
            last_ring.begin(0)
        multiply(owners, False)
    if first_ring.last == 1:
        local[3].wait()
        last_ring.begin(0)
    final_owner = first_ring.ready(first_ring.last)[0]

    lane = lax.broadcasted_iota(jnp.int32, (1, LANES), 1)
    low = lane < HEAD_DIM
    query_gain = params[0:1, :]
    sink = jnp.exp(params[1:2, :])
    pool_scale = params[2:3, :]
    pair_gain = params[3:4, :LANES]
    one_low = jnp.where(low, 1.0, 0.0)

    def spread(kv, held, count_scale):
        size = kv.shape[0]
        key_low = jnp.where(low, kv, 0.0)
        value_high = jnp.where(low, 0.0, kv)
        keys_low[held] = key_low.astype(bf16)
        keys_high[held] = pltpu.roll(key_low, HEAD_DIM, 1).astype(bf16)
        ones_low = jnp.broadcast_to(one_low * count_scale, (size, LANES)).astype(bf16)
        ones_high = jnp.broadcast_to((1.0 - one_low) * count_scale, (size, LANES)).astype(bf16)
        values_low[held, pl.ds(0, LANES)] = pltpu.roll(value_high, HEAD_DIM, 1).astype(bf16)
        values_low[held, pl.ds(LANES, LANES)] = ones_low
        values_high[held, pl.ds(0, LANES)] = value_high.astype(bf16)
        values_high[held, pl.ds(LANES, LANES)] = ones_high

    def finalise(index):
        held = aligned(index, tile)
        sums = (acc[held] + term_of(index, final_owner)).astype(bf16)
        shifted = pl.ds(pl.multiple_of(index * tile + WINDOW, WINDOW), tile)
        pool_span[shifted] = sums[:, :branch]
        kv = sums[:, mid:].astype(f32)
        squares = jnp.where(low, kv * kv, 0.0)
        scale = lax.rsqrt(jnp.sum(squares, axis=-1, keepdims=True) * (1.0 / HEAD_DIM) + epsilon)
        kv = jnp.where(low, kv * scale * pair_gain, kv).astype(bf16)
        pairs[held] = kv
        spread(kv.astype(f32), shifted, 1.0)
        wide = 2 * LANES
        for start in range(0, head_columns, wide):
            query = sums[:, branch + start : branch + start + wide].astype(f32)
            square = query * query
            upper = square.astype(bf16)
            lower = (square - upper.astype(f32)).astype(bf16)
            total = dot(upper, ones_block[...]) + dot(lower, ones_block[...])
            scale = lax.rsqrt(total * (1.0 / HEAD_DIM) + epsilon)
            queries[held, pl.ds(start, wide)] = (
                query * scale * query_gain[:, start : start + wide]
            ).astype(bf16)

    def halo_copies():
        return [
            remote(
                pairs.at[pl.ds(rows - WINDOW, WINDOW)],
                halo_pairs,
                halo_sem.at[0, 0],
                halo_sem.at[1, 0],
                "sp",
                following,
            ),
            remote(
                pool_span.at[pl.ds(WINDOW + rows - HALO_ROWS, HALO_ROWS)],
                halo_pool,
                halo_sem.at[0, 1],
                halo_sem.at[1, 1],
                "sp",
                following,
            ),
        ]

    finalise(rows // tile - 1)
    for copy in halo_copies():
        copy.start()
    last_ring.begin(1)

    @pl.loop(0, rows // tile - 1)
    def _(index):
        finalise(index)

    def pool(block):
        held = aligned(block, WINDOW)
        span_rows = pool_span[pl.ds(pl.multiple_of(block * WINDOW, WINDOW), 2 * WINDOW)]
        running = dot(band[...], span_rows)
        offset = lax.broadcasted_iota(jnp.int32, (WINDOW, 1), 0)
        position = (seq * rows + block * WINDOW + offset).astype(f32)
        counted = jnp.minimum(position + 1.0, span)
        difference = (running / counted - span_rows[WINDOW:].astype(f32)).astype(bf16)
        mapped = dot(difference, pool_map[...]) * pool_scale
        scale = lax.rsqrt(jnp.mean(mapped * mapped, axis=-1, keepdims=True) + epsilon)
        mixed[held, pl.ds(0, branch)] = (mapped * scale).astype(bf16)

    def attend(block):
        held = aligned(block, WINDOW)
        both = pl.ds(pl.multiple_of(block * WINDOW, WINDOW), 2 * WINDOW)
        key_pair = jnp.concatenate([keys_low[both], keys_high[both]], axis=0)
        value_pair = jnp.concatenate([values_low[both], values_high[both]], axis=0)
        parts, squares = [], None
        for pair in range(pairs_of_heads):
            lanes = pl.ds(pair * LANES, LANES)
            scores = lax.dot_general(
                queries[held, lanes],
                key_pair,
                (((1,), (1,)), ((), ())),
                preferred_element_type=f32,
            )
            weights = jnp.exp(scores + bias[pl.ds(pair * WINDOW, WINDOW)]).astype(bf16)
            result = dot(weights, value_pair)
            part = result[:, :LANES] / (
                result[:, LANES:] + sink[:, pair * LANES : (pair + 1) * LANES]
            )
            parts.append(part)
            squares = part * part if squares is None else squares + part * part
        mean = jnp.sum(squares, axis=-1, keepdims=True) * (1.0 / head_columns)
        scale = lax.rsqrt(mean + epsilon)
        for pair, part in enumerate(parts):
            mixed[held, pl.ds(branch + pair * LANES, LANES)] = (part * scale).astype(bf16)

    half = (blocks + 1) // 2

    @pl.loop(1, half + 1)
    def _(block):
        pool(block)
        attend(block)

    if len(last_ring.events) > 2:
        last_ring.advance()

    @pl.loop(half + 1, blocks)
    def _(block):
        pool(block)
        attend(block)

    for copy in halo_copies():
        copy.wait()
    begun = jnp.where(seq > 0, 1.0, 0.0)
    top = pl.ds(0, WINDOW)
    spread(halo_pairs[...].astype(f32) * begun, top, begun)
    pool_span[pl.ds(WINDOW - HALO_ROWS, HALO_ROWS)] = (halo_pool[...].astype(f32) * begun).astype(
        bf16
    )
    pool(0)
    attend(0)

    def output_columns(owner):
        return aligned(owner, out_width)

    def term_at(group, chunk):
        return (
            pl.ds(pl.multiple_of(group * out_rows, out_rows), out_rows),
            pl.ds(chunk * out_width, out_width),
        )

    def sum_near(chunk):
        return remote(
            normed.at[pl.ds(0, 2 * out_rows), pl.ds(chunk * out_width, out_width)],
            recv_near.at[chunk],
            sum_near_sem.at[0, chunk],
            sum_near_sem.at[1, chunk],
            "tp",
            partner,
        )

    def sum_far(chunk):
        return remote(
            send_far.at[chunk],
            recv_far.at[chunk],
            sum_far_sem.at[0, chunk],
            sum_far_sem.at[1, chunk],
            "tp",
            other,
        )

    def first(chunk, owner):
        def term(group):
            held = aligned(group, out_rows)
            return dot(mixed[held, :], last_weights[owner]).astype(bf16)

        @pl.loop(0, 2)
        def _(pick):
            normed[term_at(pick, chunk)] = term(jnp.where(pick == 0, across, partner))

        sum_near(chunk).start()

        @pl.loop(0, 2)
        def _(pick):
            normed[term_at(pick + 2, chunk)] = term(jnp.where(pick == 0, other, me))

    def second(chunk):
        sum_near(chunk).wait_recv()
        send_far[chunk] = (
            normed[term_at(2, chunk)].astype(f32) + recv_near[chunk, :out_rows].astype(f32)
        ).astype(bf16)
        sum_far(chunk).start()

    def third(chunk, owner):
        sum_far(chunk).wait_recv()
        out[:, output_columns(owner)] = (
            normed[term_at(3, chunk)].astype(f32)
            + recv_near[chunk, out_rows:].astype(f32)
            + recv_far[chunk].astype(f32)
        ).astype(bf16)

    owners = [last_ring.owner(0)]
    first(0, owners[0])
    second(0)
    finished = 0
    for step in range(1, last_ring.last + 1):
        fresh = last_ring.ready(step)
        start = len(owners)
        for extra, owner in enumerate(fresh):
            first(start + extra, owner)
        for extra in range(len(fresh)):
            second(start + extra)
        while finished < start:
            third(finished, owners[finished])
            finished += 1
        owners += fresh
    while finished < count:
        third(finished, owners[finished])
        finished += 1
    first_ring.sent()
    last_ring.sent()
    for chunk in range(count):
        sum_near(chunk).wait_send()
        sum_far(chunk).wait_send()


def layer(tokens, w_pool_in, w_query, w_key_t, w_value_t, pool_map, w_out, gain, params):
    count = lax.axis_size("sp")
    rows, width = tokens.shape
    depth, branch = w_pool_in.shape
    head_columns = w_query.shape[1]
    features = width * lax.axis_size("tp")
    mix, out_width = w_out.shape
    out_rows = rows // lax.axis_size("tp")
    dma = pltpu.SemaphoreType.DMA
    last = count // 2
    vmem = pl.BlockSpec(memory_space=pltpu.VMEM)
    hbm = pl.BlockSpec(memory_space=pltpu.HBM)
    flops = 2 * rows * features * (branch + head_columns + LANES) + 2 * rows * mix * count * out_width
    return pl.pallas_call(
        functools.partial(layer_kernel, count),
        out_shape=jax.ShapeDtypeStruct((out_rows, count * out_width), bf16),
        in_specs=[hbm, hbm, hbm, vmem, vmem, vmem, hbm, vmem, vmem],
        out_specs=vmem,
        scratch_shapes=[
            pltpu.VMEM((rows, features), bf16),
            pltpu.VMEM((features, branch + head_columns + LANES), bf16),
            pltpu.VMEM((count, mix, out_width), bf16),
            pltpu.VMEM((rows, branch + head_columns + LANES), f32),
            pltpu.VMEM((rows, head_columns), bf16),
            pltpu.VMEM((WINDOW + rows, LANES), bf16),
            pltpu.VMEM((WINDOW + rows, LANES), bf16),
            pltpu.VMEM((WINDOW + rows, 2 * LANES), bf16),
            pltpu.VMEM((WINDOW + rows, 2 * LANES), bf16),
            pltpu.VMEM((WINDOW + rows, branch), bf16),
            pltpu.VMEM((rows, LANES), bf16),
            pltpu.VMEM((rows, mix), bf16),
            pltpu.VMEM((head_columns // LANES * WINDOW, 4 * WINDOW), f32),
            pltpu.VMEM((WINDOW, 2 * WINDOW), bf16),
            pltpu.VMEM((2 * LANES, 2 * LANES), bf16),
            pltpu.VMEM((WINDOW, LANES), bf16),
            pltpu.VMEM((HALO_ROWS, branch), bf16),
            pltpu.VMEM((count, 2 * out_rows, out_width), bf16),
            pltpu.VMEM((count, out_rows, out_width), bf16),
            pltpu.VMEM((count, out_rows, out_width), bf16),
            dma((4,)),
            dma((2, last, 2)),
            dma((2, last, 2)),
            dma((2, last, 2)),
            dma((2, last, 2)),
            dma((2,)),
            dma((2, TOKEN_CHUNKS)),
            dma((2, TOKEN_CHUNKS)),
            dma((2, 2)),
            dma((2, count)),
            dma((2, count)),
        ],
        compiler_params=pltpu.CompilerParams(
            collective_id=0, has_side_effects=True, vmem_limit_bytes=63 * 1024 * 1024
        ),
        cost_estimate=pl.CostEstimate(
            flops=flops, bytes_accessed=4 * rows * width, transcendentals=0
        ),
    )(tokens, w_pool_in, w_query, w_key_t, w_value_t, pool_map, w_out, gain, params)


def local(
    tokens,
    norm_gain,
    w_pool_in,
    w_query,
    w_key,
    w_value,
    pool_map,
    pool_scale,
    q_gain,
    k_gain,
    sinks,
    w_out,
):
    head_columns = w_query.shape[1]
    params = jnp.stack(
        [
            jnp.tile(q_gain * HEAD_DIM**-0.5, head_columns // HEAD_DIM),
            jnp.repeat(sinks, HEAD_DIM),
            pool_scale,
            jnp.tile(k_gain, head_columns // HEAD_DIM),
        ]
    )
    return layer(
        tokens,
        w_pool_in,
        w_query,
        w_key.T,
        w_value.T,
        pool_map[0],
        w_out,
        norm_gain[None],
        params,
    )


def solution(mesh):
    in_specs = (
        P("sp", "tp"),
        P(),
        P("sp", "tp"),
        P("sp", "tp"),
        P("sp", "tp"),
        P("sp", "tp"),
        P("tp", None, None),
        P("tp"),
        P(),
        P(),
        P("tp"),
        P("tp", "sp"),
    )
    out_specs = P(("sp", "tp"), None)
    return jax.shard_map(local, mesh=mesh, in_specs=in_specs, out_specs=out_specs, check_vma=False)
```

time: 289 us -> 197 us (0.68)
  waiting for transfers between devices: 35.8 us -> 0 us
  Pallas kernels: 160 us -> 190 us
  local copies, waits for them, and re-layouts: 31.1 us -> 4.75 us
  matrix products: 22.6 us -> 0 us
  other arithmetic: 17.1 us -> 1.95 us
  between operations: 13.8 us -> 0.01 us
  starting transfers between devices: 6.84 us -> 0 us
    all_gather x1 -> x0, waiting for transfers between devices: 35.7 us -> none  [local(): head_columns = lax.all_gather(w_head, 'sp', axis=1, tiled=True)]
    pallas_call x2 -> x1, Pallas kernels: 160 us -> 190 us  [layer(): pl.pallas_call(functools.partial(layer_kernel, count), out_shape=jax.Shap...]
    dot_general x4 -> x0, matrix products: 22.6 us -> none  [the longest x1 15.2 us: local(): jnp.dot(normed, all_weights, preferred_element_type=jnp.float32)]
    ppermute x2 -> x0, starting transfers between devices: 6.84 us -> none  [passed_along(): lax.ppermute(value, axis, [(source, source + steps) for source in range(f...]
    reduce_sum x3 -> x0, other arithmetic: 5.67 us -> none  [rms_scale(): jnp.mean(values * values, axis=-1, keepdims=True) + epsilon]
    slice x5 -> x0, local copies, waits for them, and re-layouts: 5.66 us -> none  [the longest x1 2.64 us: local(): pool_sum, query_sum = (sums[:, :pool_end], sums[:, pool_end:query_end])]
    unnamed x40 -> x1, local copies, waits for them, and re-layouts: 8.32 us -> 3.13 us
    reshape x6 -> x0, local copies, waits for them, and re-layouts: 4.76 us -> none  [the longest x1 1.93 us: local(): attended.reshape(tok_rows, local_groups, GROUP_WIDTH)]
  transfers between devices with their start and end apart: 3 -> 0, of which waited for: 1 -> 0; matrix products, arithmetic and copies ran while one was open for 13% -> 0% of each run, Pallas kernels for 0% -> 0%
where the time goes in v1:
time: 197 us; the launch traced here: 196 us
  Pallas kernels  190 us (96%)
  local copies, waits for them, and re-layouts  4.75 us (2%)
    pallas_call x1, Pallas kernels, layer(): pl.pallas_call(functools.partial(layer_kernel, count), out_shape=jax.Shap...  190 us

profile of v1, /device:TPU:1, one launch (start us, length us, event | category | flops | bytes accessed | tf_op | source)
XLA Modules:
  0.0 196.4 jit_solution(18418771932238720138)
XLA Ops:
  0.0 0.7 broadcast_multiply_fusion
  0.7 0.1 stack_tile.6
  0.7 0.7 tile.5
  1.4 0.1 stack_tile.7
  1.5 0.7 broadcast_in_dim.7
  2.2 0.1 stack_reshape.3
  2.3 1.3 pad_maximum_fusion.params
  3.6 189.7 %shard_map.118 = bf16[256,4096]{1,0:T(8,128)(2,1)} custom-call(bf16[1024,1024]{1,0:T(8,128)(2,1)} %tokens.1, bf16[512,512]{1,0:T(8,128)(2,1)} %w_pool_in.1, bf16[512,512]{1,0:T(8,128)(2,1)} %w_query.1, bf16[64,512]{1,0:T(8,128)(2,1)} %bitcast.7, bf16[64,512]{1,0:T(8,128)(2,1)} %bitcast.8, bf16[512,512]{1,0:T(8,128)(2,1)} %bitcast.6, ...), custom_call_target="tpu_custom_call" | custom-call | flops 18253611008 | bytes 4194304 | tf_op jit(solution)/shard_map/pallas_call | solution.py:552
  193.3 3.1 %copy.14 = bf16[256,4096]{1,0:T(8,128)(2,1)} copy(bf16[256,4096]{1,0:T(8,128)(2,1)} %shard_map.118) | data formatting | bytes 4194304
  (1 shorter events, 0.0 us)

commit v2 on v1

--- a/solution.py
+++ b/solution.py
@@ -40,7 +40,10 @@
         pl.semaphore_signal(
             barrier, inc=1, device_id={axis: target}, device_id_type=pl.DeviceIdType.MESH
         )
-    pl.semaphore_wait(barrier, len(targets))
+
+
+def await_greetings(count):
+    pl.semaphore_wait(pltpu.get_barrier_semaphore(), count)
 
 
 def remote(source, target, send_sem, recv_sem, axis, device):
@@ -63,8 +66,8 @@
 
 
 class Ring:
-    def __init__(self, count, block_at, send, recv):
-        self.count, self.last = count, count // 2
+    def __init__(self, count, block_at, send, recv, pieces):
+        self.count, self.last, self.pieces = count, count // 2, pieces
         self.place = ring_place(lax.axis_index("sp"), count)
         self.targets = (
             ring_device(self.place + 1, count),
@@ -73,50 +76,55 @@
         self.block_at, self.send, self.recv = block_at, send, recv
         self.started = []
         self.events = [(step, part) for step in range(1, self.last) for part in range(2)]
-        self.events.append((self.last, None))
+        self.events += [(self.last, piece) for piece in range(pieces)]
         self.done = 0
 
     def owner(self, distance):
         return ring_device(self.place - distance, self.count)
 
-    def copy(self, step, way, part):
-        block = self.block_at(self.owner((1 - 2 * way) * (step - 1)), part)
+    def copy(self, step, way, slot):
+        owner = self.owner((1 - 2 * way) * (step - 1))
+        if step < self.last:
+            block = self.block_at(owner, slot, 0, 1)
+        else:
+            block = self.block_at(owner, way, slot, self.pieces)
         return remote(
             block,
             block,
-            self.send.at[way, step - 1, part],
-            self.recv.at[way, step - 1, part],
+            self.send.at[way, step - 1, slot],
+            self.recv.at[way, step - 1, slot],
             "sp",
             self.targets[way],
         )
 
     def start(self, step, way, part):
-        self.copy(step, way, part).start()
-        self.started.append((step, way, part))
+        if step < self.last:
+            slots = [part]
+        else:
+            slots = range(self.pieces) if part == way else []
+        for slot in slots:
+            self.copy(step, way, slot).start()
+            self.started.append((step, way, slot))
 
     def begin(self, part):
         for way in range(2):
-            if self.last > 1 or part == way:
-                self.start(1, way, part)
+            self.start(1, way, part)
 
     def advance(self):
-        step, part = self.events[self.done]
+        step, slot = self.events[self.done]
         self.done += 1
         for way in range(2):
-            held = way if part is None else part
-            self.copy(step, way, held).wait_recv()
-            if step < self.last and (step + 1 < self.last or held == way):
-                self.start(step + 1, way, held)
-
-    def ready(self, step):
-        target = len(self.events) if step == self.last else 2 * step
-        while self.done < target:
+            self.copy(step, way, slot).wait_recv()
+            if step < self.last:
+                self.start(step + 1, way, slot)
+
+    def upto(self, event):
+        while self.done <= event:
             self.advance()
-        return [self.owner(step)] if step == self.last else [self.owner(step), self.owner(-step)]
 
     def sent(self):
-        for step, way, part in self.started:
-            self.copy(step, way, part).wait_send()
+        for step, way, slot in self.started:
+            self.copy(step, way, slot).wait_send()
 
 
 def layer_kernel(
@@ -128,8 +136,11 @@
     w_value_t,
     pool_map,
     w_out,
-    gain,
-    params,
+    gain_in,
+    pool_scale_in,
+    q_gain_in,
+    k_gain_in,
+    sinks_in,
     out,
     normed,
     first_weights,
@@ -151,6 +162,14 @@
     recv_near,
     send_far,
     recv_far,
+    key_value,
+    pool_maps,
+    gain,
+    pool_scales,
+    q_gain,
+    k_gain,
+    sinks,
+    head_rows,
     local_sem,
     first_send,
     first_recv,
@@ -177,50 +196,66 @@
     mix = w_out.shape[0]
     pairs_of_heads = head_columns // LANES
 
-    def first_block(owner, part):
+    halves = out_width % (2 * LANES) == 0
+    pieces = 2 if out_width % (4 * LANES) == 0 else 1
+
+    def first_block(owner, part, piece, pieces):
+        size = depth // 2 // pieces
         return first_weights.at[
-            pl.ds(pl.multiple_of(owner * depth + part * (depth // 2), depth // 2), depth // 2)
+            pl.ds(pl.multiple_of(owner * depth + part * (depth // 2) + piece * size, size), size)
         ]
 
-    def last_block(owner, part):
-        return last_weights.at[owner, pl.ds(part * (mix // 2), mix // 2)]
-
-    first_ring = Ring(count, first_block, first_send, first_recv)
-    last_ring = Ring(count, last_block, last_send, last_recv)
+    def last_block(owner, part, piece, pieces):
+        if halves:
+            size = out_width // 2 // pieces
+            return last_weights.at[
+                owner, :, pl.ds(part * (out_width // 2) + piece * size, size)
+            ]
+        size = mix // 2 // pieces
+        return last_weights.at[owner, pl.ds(part * (mix // 2) + piece * size, size)]
+
+    first_ring = Ring(count, first_block, first_send, first_recv, 1)
+    last_ring = Ring(count, last_block, last_send, last_recv, pieces)
     following = (seq + 1) % count
-    preceding = (seq + count - 1) % count
 
     def columns(owner):
         return aligned(owner, width)
 
     own_rows = aligned(seq, depth)
+    greetings = [
+        ("sp", first_ring.targets[0]),
+        ("sp", first_ring.targets[1]),
+        ("tp", partner),
+        ("tp", other),
+    ]
+    greet(greetings)
     local = [
         pltpu.make_async_copy(source, target, local_sem.at[index])
         for index, (source, target) in enumerate(
             [
+                (w_key_t, key_value.at[pl.ds(0, HEAD_DIM)]),
+                (w_value_t, key_value.at[pl.ds(HEAD_DIM, HEAD_DIM)]),
                 (w_pool_in, first_weights.at[own_rows, pl.ds(0, branch)]),
                 (w_query, first_weights.at[own_rows, pl.ds(branch, head_columns)]),
                 (tokens, normed.at[:, columns(me)]),
                 (w_out, last_weights.at[seq]),
+                (pool_map, pool_maps),
+                (gain_in, gain),
+                (pool_scale_in, pool_scales),
+                (q_gain_in, q_gain),
+                (k_gain_in, k_gain),
+                (sinks_in, sinks),
             ]
         )
     ]
     for copy in local:
         copy.start()
-    key_value = jnp.concatenate([w_key_t[...], w_value_t[...]], axis=0).astype(f32)
-    first_weights[own_rows, pl.ds(mid, LANES)] = key_value.T.astype(bf16)
-    greet(
-        [
-            ("sp", first_ring.targets[0]),
-            ("sp", first_ring.targets[1]),
-            ("sp", following),
-            ("sp", preceding),
-            ("tp", partner),
-            ("tp", other),
-        ]
-    )
     local[0].wait()
     local[1].wait()
+    first_weights[own_rows, pl.ds(mid, LANES)] = key_value[...].astype(f32).T.astype(bf16)
+    await_greetings(len(greetings))
+    local[2].wait()
+    local[3].wait()
     first_ring.begin(0)
     first_ring.begin(1)
 
@@ -275,7 +310,20 @@
             scale = lax.rsqrt(jnp.mean(values * values, axis=-1, keepdims=True) + epsilon)
             normed[held] = (values * scale * gain[...]).astype(bf16)
 
-    local[2].wait()
+    lane = lax.broadcasted_iota(jnp.int32, (1, LANES), 1)
+    low = lane < HEAD_DIM
+    for copy in local[4:]:
+        copy.wait()
+    head_rows[...] = jnp.zeros(head_rows.shape, f32)
+    head_rows[pl.ds(0, 1), pl.ds(0, HEAD_DIM)] = q_gain[...] * HEAD_DIM**-0.5
+    head_rows[pl.ds(1, 1), pl.ds(0, HEAD_DIM)] = k_gain[...]
+    once = head_rows[pl.ds(0, 1), :]
+    head_rows[pl.ds(0, 1), :] = once + pltpu.roll(once, HEAD_DIM, 1)
+    for pair in range(pairs_of_heads):
+        head_rows[pl.ds(2 + pair, 1), :] = jnp.exp(
+            jnp.where(low, sinks[2 * pair], sinks[2 * pair + 1])
+        )
+
     for chunk in range(TOKEN_CHUNKS):
         far_copy(chunk).wait_recv()
         pass_copy(chunk).start()
@@ -305,22 +353,15 @@
 
     multiply([first_ring.owner(0)], True)
     for step in range(1, first_ring.last):
-        owners = first_ring.ready(step)
+        first_ring.upto(2 * step - 1)
         if step == first_ring.last - 1:
-            local[3].wait()
             last_ring.begin(0)
-        multiply(owners, False)
+        multiply([first_ring.owner(step), first_ring.owner(-step)], False)
     if first_ring.last == 1:
-        local[3].wait()
         last_ring.begin(0)
-    final_owner = first_ring.ready(first_ring.last)[0]
-
-    lane = lax.broadcasted_iota(jnp.int32, (1, LANES), 1)
-    low = lane < HEAD_DIM
-    query_gain = params[0:1, :]
-    sink = jnp.exp(params[1:2, :])
-    pool_scale = params[2:3, :]
-    pair_gain = params[3:4, :LANES]
+    first_ring.upto(len(first_ring.events) - 1)
+    final_owner = first_ring.owner(first_ring.last)
+
     one_low = jnp.where(low, 1.0, 0.0)
 
     def spread(kv, held, count_scale):
@@ -344,10 +385,12 @@
         kv = sums[:, mid:].astype(f32)
         squares = jnp.where(low, kv * kv, 0.0)
         scale = lax.rsqrt(jnp.sum(squares, axis=-1, keepdims=True) * (1.0 / HEAD_DIM) + epsilon)
-        kv = jnp.where(low, kv * scale * pair_gain, kv).astype(bf16)
+        kv = jnp.where(low, kv * scale * head_rows[pl.ds(1, 1), :], kv).astype(bf16)
         pairs[held] = kv
         spread(kv.astype(f32), shifted, 1.0)
         wide = 2 * LANES
+        gain_row = head_rows[pl.ds(0, 1), :]
+        query_gain = jnp.concatenate([gain_row, gain_row], axis=1)
         for start in range(0, head_columns, wide):
             query = sums[:, branch + start : branch + start + wide].astype(f32)
             square = query * query
@@ -356,7 +399,7 @@
             total = dot(upper, ones_block[...]) + dot(lower, ones_block[...])
             scale = lax.rsqrt(total * (1.0 / HEAD_DIM) + epsilon)
             queries[held, pl.ds(start, wide)] = (
-                query * scale * query_gain[:, start : start + wide]
+                query * scale * query_gain
             ).astype(bf16)
 
     def halo_copies():
@@ -396,7 +439,7 @@
         position = (seq * rows + block * WINDOW + offset).astype(f32)
         counted = jnp.minimum(position + 1.0, span)
         difference = (running / counted - span_rows[WINDOW:].astype(f32)).astype(bf16)
-        mapped = dot(difference, pool_map[...]) * pool_scale
+        mapped = dot(difference, pool_maps[...]) * pool_scales[...]
         scale = lax.rsqrt(jnp.mean(mapped * mapped, axis=-1, keepdims=True) + epsilon)
         mixed[held, pl.ds(0, branch)] = (mapped * scale).astype(bf16)
 
@@ -417,7 +460,7 @@
             weights = jnp.exp(scores + bias[pl.ds(pair * WINDOW, WINDOW)]).astype(bf16)
             result = dot(weights, value_pair)
             part = result[:, :LANES] / (
-                result[:, LANES:] + sink[:, pair * LANES : (pair + 1) * LANES]
+                result[:, LANES:] + head_rows[pl.ds(2 + pair, 1), :]
             )
             parts.append(part)
             squares = part * part if squares is None else squares + part * part
@@ -434,7 +477,7 @@
         attend(block)
 
     if len(last_ring.events) > 2:
-        last_ring.advance()
+        last_ring.upto(0)
 
     @pl.loop(half + 1, blocks)
     def _(block):
@@ -452,91 +495,164 @@
     pool(0)
     attend(0)
 
-    def output_columns(owner):
-        return aligned(owner, out_width)
-
-    def term_at(group, chunk):
-        return (
-            pl.ds(pl.multiple_of(group * out_rows, out_rows), out_rows),
-            pl.ds(chunk * out_width, out_width),
-        )
-
-    def sum_near(chunk):
-        return remote(
-            normed.at[pl.ds(0, 2 * out_rows), pl.ds(chunk * out_width, out_width)],
-            recv_near.at[chunk],
-            sum_near_sem.at[0, chunk],
-            sum_near_sem.at[1, chunk],
-            "tp",
-            partner,
-        )
-
-    def sum_far(chunk):
-        return remote(
-            send_far.at[chunk],
-            recv_far.at[chunk],
-            sum_far_sem.at[0, chunk],
-            sum_far_sem.at[1, chunk],
-            "tp",
-            other,
-        )
-
-    def first(chunk, owner):
-        def term(group):
-            held = aligned(group, out_rows)
-            return dot(mixed[held, :], last_weights[owner]).astype(bf16)
-
-        @pl.loop(0, 2)
-        def _(pick):
-            normed[term_at(pick, chunk)] = term(jnp.where(pick == 0, across, partner))
-
-        sum_near(chunk).start()
-
-        @pl.loop(0, 2)
-        def _(pick):
-            normed[term_at(pick + 2, chunk)] = term(jnp.where(pick == 0, other, me))
-
-    def second(chunk):
-        sum_near(chunk).wait_recv()
-        send_far[chunk] = (
-            normed[term_at(2, chunk)].astype(f32) + recv_near[chunk, :out_rows].astype(f32)
-        ).astype(bf16)
-        sum_far(chunk).start()
-
-    def third(chunk, owner):
-        sum_far(chunk).wait_recv()
-        out[:, output_columns(owner)] = (
-            normed[term_at(3, chunk)].astype(f32)
-            + recv_near[chunk, out_rows:].astype(f32)
-            + recv_far[chunk].astype(f32)
-        ).astype(bf16)
-
-    owners = [last_ring.owner(0)]
-    first(0, owners[0])
-    second(0)
-    finished = 0
-    for step in range(1, last_ring.last + 1):
-        fresh = last_ring.ready(step)
-        start = len(owners)
-        for extra, owner in enumerate(fresh):
-            first(start + extra, owner)
-        for extra in range(len(fresh)):
-            second(start + extra)
-        while finished < start:
-            third(finished, owners[finished])
-            finished += 1
-        owners += fresh
-    while finished < count:
-        third(finished, owners[finished])
-        finished += 1
+    half_width = out_width // 2
+    size_of = half_width if halves else out_width
+    batches = []
+    if halves:
+        batches.append((-1, 2, size_of, lambda unit: (last_ring.owner(0), unit * half_width)))
+    else:
+        batches.append((-1, 1, size_of, lambda unit: (last_ring.owner(0), 0)))
+    for event, (step, slot) in enumerate(last_ring.events):
+        final = step == last_ring.last
+        if not halves:
+            if slot < (pieces if final else 2) - 1:
+                continue
+            if final:
+                batches.append((event, 1, size_of, lambda unit: (last_ring.owner(last_ring.last), 0)))
+            else:
+                batches.append(
+                    (
+                        event,
+                        2,
+                        size_of,
+                        lambda unit, step=step: (last_ring.owner((1 - 2 * unit) * step), 0),
+                    )
+                )
+        elif final:
+            batches.append(
+                (
+                    event,
+                    2,
+                    size_of // pieces,
+                    lambda unit, slot=slot: (
+                        last_ring.owner(last_ring.last),
+                        unit * half_width + slot * (half_width // pieces),
+                    ),
+                )
+            )
+        else:
+            batches.append(
+                (
+                    event,
+                    2,
+                    size_of,
+                    lambda unit, step=step, slot=slot: (
+                        last_ring.owner((1 - 2 * unit) * step),
+                        slot * half_width,
+                    ),
+                )
+            )
+
+    class Batch:
+        def __init__(self, first_unit, base, event, units, size, place):
+            self.first_unit, self.base, self.event = first_unit, base, event
+            self.units, self.size, self.place = units, size, place
+
+        def lanes(self, unit):
+            step = min(self.size, LANES)
+            return pl.ds(pl.multiple_of(self.base + unit * self.size, step), self.size)
+
+        def group(self, slot):
+            return pl.ds(slot * out_rows, out_rows)
+
+        def near(self, unit, pick):
+            return remote(
+                normed.at[self.group(pick), self.lanes(unit)],
+                recv_near.at[self.group(pick), self.lanes(unit)],
+                sum_near_sem.at[0, pick, self.first_unit + unit],
+                sum_near_sem.at[1, pick, self.first_unit + unit],
+                "tp",
+                partner,
+            )
+
+        def far(self, unit):
+            return remote(
+                send_far.at[:, self.lanes(unit)],
+                recv_far.at[:, self.lanes(unit)],
+                sum_far_sem.at[0, self.first_unit + unit],
+                sum_far_sem.at[1, self.first_unit + unit],
+                "tp",
+                other,
+            )
+
+        def term(self, unit, slot, target):
+            owner, start = self.place(unit)
+            if not isinstance(start, int):
+                start = pl.multiple_of(start, min(self.size, LANES))
+            value = dot(
+                mixed[aligned(target, out_rows), :],
+                last_weights[owner, :, pl.ds(start, self.size)],
+            )
+            normed[self.group(slot), self.lanes(unit)] = value.astype(bf16)
+
+        def early(self):
+            @pl.loop(0, self.units)
+            def _(unit):
+                self.term(unit, 0, across)
+                self.near(unit, 0).start()
+                self.term(unit, 2, other)
+
+        def middle(self):
+            @pl.loop(0, self.units)
+            def _(unit):
+                self.near(unit, 0).wait_recv()
+                lanes = self.lanes(unit)
+                send_far[:, lanes] = (
+                    normed[self.group(2), lanes].astype(f32)
+                    + recv_near[self.group(0), lanes].astype(f32)
+                ).astype(bf16)
+                self.far(unit).start()
+
+        def late(self):
+            @pl.loop(0, self.units)
+            def _(unit):
+                self.term(unit, 1, partner)
+                self.near(unit, 1).start()
+                self.term(unit, 3, me)
+
+        def finish(self):
+            @pl.loop(0, self.units)
+            def _(unit):
+                self.near(unit, 1).wait_recv()
+                self.far(unit).wait_recv()
+                lanes = self.lanes(unit)
+                owner, start = self.place(unit)
+                target = pl.ds(
+                    pl.multiple_of(owner * out_width + start, min(self.size, LANES)), self.size
+                )
+                out[:, target] = (
+                    normed[self.group(3), lanes].astype(f32)
+                    + recv_near[self.group(1), lanes].astype(f32)
+                    + recv_far[:, lanes].astype(f32)
+                ).astype(bf16)
+
+        def sent(self):
+            @pl.loop(0, self.units)
+            def _(unit):
+                self.near(unit, 0).wait_send()
+                self.near(unit, 1).wait_send()
+                self.far(unit).wait_send()
+
+    unit, base, built = 0, 0, []
+    for event, units, size, place in batches:
+        batch = Batch(unit, base, event, units, size, place)
+        last_ring.upto(event)
+        batch.early()
+        batch.middle()
+        batch.late()
+        if len(built) > 1:
+            built[-2].finish()
+        built.append(batch)
+        unit, base = unit + units, base + units * size
+    for batch in built[-2:]:
+        batch.finish()
     first_ring.sent()
     last_ring.sent()
-    for chunk in range(count):
-        sum_near(chunk).wait_send()
-        sum_far(chunk).wait_send()
-
-
-def layer(tokens, w_pool_in, w_query, w_key_t, w_value_t, pool_map, w_out, gain, params):
+    for batch in built:
+        batch.sent()
+
+
+def layer(tokens, w_pool_in, w_query, w_key_t, w_value_t, pool_map, w_out, *rows_in):
     count = lax.axis_size("sp")
     rows, width = tokens.shape
     depth, branch = w_pool_in.shape
@@ -544,16 +660,17 @@
     features = width * lax.axis_size("tp")
     mix, out_width = w_out.shape
     out_rows = rows // lax.axis_size("tp")
+    out_columns = count * out_width
     dma = pltpu.SemaphoreType.DMA
     last = count // 2
-    vmem = pl.BlockSpec(memory_space=pltpu.VMEM)
+    units = 4 * count
     hbm = pl.BlockSpec(memory_space=pltpu.HBM)
-    flops = 2 * rows * features * (branch + head_columns + LANES) + 2 * rows * mix * count * out_width
+    flops = 2 * rows * features * (branch + head_columns + LANES) + 2 * rows * mix * out_columns
     return pl.pallas_call(
         functools.partial(layer_kernel, count),
-        out_shape=jax.ShapeDtypeStruct((out_rows, count * out_width), bf16),
-        in_specs=[hbm, hbm, hbm, vmem, vmem, vmem, hbm, vmem, vmem],
-        out_specs=vmem,
+        out_shape=pltpu.VMEM((out_rows, out_columns), bf16),
+        in_specs=[hbm] * 12,
+        out_specs=pl.BlockSpec(memory_space=pltpu.VMEM),
         scratch_shapes=[
             pltpu.VMEM((rows, features), bf16),
             pltpu.VMEM((features, branch + head_columns + LANES), bf16),
@@ -572,10 +689,18 @@
             pltpu.VMEM((2 * LANES, 2 * LANES), bf16),
             pltpu.VMEM((WINDOW, LANES), bf16),
             pltpu.VMEM((HALO_ROWS, branch), bf16),
-            pltpu.VMEM((count, 2 * out_rows, out_width), bf16),
-            pltpu.VMEM((count, out_rows, out_width), bf16),
-            pltpu.VMEM((count, out_rows, out_width), bf16),
-            dma((4,)),
+            pltpu.VMEM((2 * out_rows, out_columns), bf16),
+            pltpu.VMEM((out_rows, out_columns), bf16),
+            pltpu.VMEM((out_rows, out_columns), bf16),
+            pltpu.VMEM((2 * HEAD_DIM, depth), bf16),
+            pltpu.VMEM((branch, branch), bf16),
+            pltpu.VMEM((1, features), f32),
+            pltpu.VMEM((1, branch), f32),
+            pltpu.VMEM((1, HEAD_DIM), f32),
+            pltpu.VMEM((1, HEAD_DIM), f32),
+            pltpu.SMEM((GROUP,), f32),
+            pltpu.VMEM((8, LANES), f32),
+            dma((12,)),
             dma((2, last, 2)),
             dma((2, last, 2)),
             dma((2, last, 2)),
@@ -584,16 +709,16 @@
             dma((2, TOKEN_CHUNKS)),
             dma((2, TOKEN_CHUNKS)),
             dma((2, 2)),
-            dma((2, count)),
-            dma((2, count)),
+            dma((2, 2, units)),
+            dma((2, units)),
         ],
         compiler_params=pltpu.CompilerParams(
-            collective_id=0, has_side_effects=True, vmem_limit_bytes=63 * 1024 * 1024
+            collective_id=0, has_side_effects=True, vmem_limit_bytes=58 * 1024 * 1024
         ),
         cost_estimate=pl.CostEstimate(
             flops=flops, bytes_accessed=4 * rows * width, transcendentals=0
         ),
-    )(tokens, w_pool_in, w_query, w_key_t, w_value_t, pool_map, w_out, gain, params)
+    )(tokens, w_pool_in, w_query, w_key_t, w_value_t, pool_map, w_out, *rows_in)
 
 
 def local(
@@ -610,15 +735,6 @@
     sinks,
     w_out,
 ):
-    head_columns = w_query.shape[1]
-    params = jnp.stack(
-        [
-            jnp.tile(q_gain * HEAD_DIM**-0.5, head_columns // HEAD_DIM),
-            jnp.repeat(sinks, HEAD_DIM),
-            pool_scale,
-            jnp.tile(k_gain, head_columns // HEAD_DIM),
-        ]
-    )
     return layer(
         tokens,
         w_pool_in,
@@ -628,7 +744,10 @@
         pool_map[0],
         w_out,
         norm_gain[None],
-        params,
+        pool_scale[None],
+        q_gain[None],
+        k_gain[None],
+        sinks,
     )
 
 

time: 197 us -> 185 us (0.939)
  Pallas kernels: 190 us -> 183 us
  local copies, waits for them, and re-layouts: 4.75 us -> 1.32 us
    pallas_call x1, Pallas kernels: 190 us -> 183 us  [layer(): pl.pallas_call(functools.partial(layer_kernel, count), out_shape=pltpu.VM...]
where the time goes in v2:
time: 185 us
  Pallas kernels  183 us (99%)
    pallas_call x1, Pallas kernels, layer(): pl.pallas_call(functools.partial(layer_kernel, count), out_shape=pltpu.VM...  183 us

profile of v2, /device:TPU:1, one launch (start us, length us, event | category | flops | bytes accessed | tf_op | source)
XLA Modules:
  0.0 184.6 jit_solution(3283300755622146430)
XLA Ops:
  0.0 183.3 %shard_map.118 = bf16[256,4096]{1,0:T(8,128)(2,1)S(1)} custom-call(bf16[1024,1024]{1,0:T(8,128)(2,1)} %tokens.1, bf16[512,512]{1,0:T(8,128)(2,1)} %w_pool_in.1, bf16[512,512]{1,0:T(8,128)(2,1)} %w_query.1, bf16[64,512]{1,0:T(8,128)(2,1)} %bitcast.8, bf16[64,512]{1,0:T(8,128)(2,1)} %bitcast.9, bf16[512,512]{1,0:T(8,128)(2,1)} %bitcast.7, ...), custom_call_target="tpu_custom_call" | custom-call | flops 18253611008 | bytes 4194304 | tf_op jit(solution)/shard_map/pallas_call | solution.py:669
  183.3 1.3 copy.14

commit v3 on v2

v3 whole, which is shorter than its diff:
```python
import functools

import jax
import jax.numpy as jnp
from jax import lax
from jax.experimental import pallas as pl
from jax.experimental.pallas import tpu as pltpu
from jax.sharding import PartitionSpec as P

HEAD_DIM = 64
GROUP = 8
WINDOW = 128
Q_HEADS = 32
LANES = 128
TOKEN_CHUNKS = 4
HALO_ROWS = 16
MASKED = -1e30

epsilon = 1e-06
bf16, f32 = jnp.bfloat16, jnp.float32


def aligned(index, size):
    return pl.ds(pl.multiple_of(index * size, size), size)


def dot(left, right):
    return jnp.dot(left, right, preferred_element_type=f32)


class Place:
    def __init__(self, count):
        self.planes = count // 2
        self.sp, self.tp = lax.axis_index("sp"), lax.axis_index("tp")
        self.z, self.y = self.sp // 2, self.sp % 2
        self.x, self.c = self.tp // 2, self.tp % 2
        self.home = self.y == self.c
        self.rows_of, self.group = 2 * self.z + self.c, 2 * self.x + self.y

    def sibling(self):
        return {"tp": 2 * self.x + 1 - self.c}

    def along_x(self, core):
        return {"tp": 2 * (1 - self.x) + core}

    def along_y(self, core):
        return {"sp": 2 * self.z + 1 - self.y, "tp": 2 * self.x + core}

    def along_z(self, way):
        return {"sp": self.sp + 2 - 4 * way}

    def source(self, way, steps):
        return self.z - steps if way == 0 else self.z + steps

    def has(self, way, steps):
        return self.z >= steps if way == 0 else self.z + steps < self.planes

    def passes(self, way):
        return self.z + 1 < self.planes if way == 0 else self.z > 0


def remote(source, target, send_sem, recv_sem, device):
    return pltpu.make_async_remote_copy(
        src_ref=source,
        dst_ref=target,
        send_sem=send_sem,
        recv_sem=recv_sem,
        device_id=device,
        device_id_type=pl.DeviceIdType.MESH,
    )


class Chain:
    def __init__(self, place, shard, own_first, sems):
        self.place, self.shard, self.own_first = place, shard, own_first
        self.up_send, self.up_recv, self.pair_send, self.pair_recv, self.edge = sems
        self.events = [(step, slot) for step in range(place.planes) for slot in range(2)]
        self.done, self.whole = 0, set()

    def block(self, plane, slot, half):
        side = slot if not self.own_first else (self.place.y + slot) % 2
        return self.shard(2 * plane + side, half)

    def hop(self, way, step, slot):
        held = self.block(self.place.source(way, step), slot, self.place.c)
        return remote(
            held,
            held,
            self.up_send.at[way, step, slot],
            self.up_recv.at[way, step, slot],
            self.place.along_z(way),
        )

    def pair(self, way, step, slot):
        held = self.block(self.place.source(way, step), slot, self.place.c)
        return remote(
            held,
            held,
            self.pair_send.at[way, step, slot],
            self.pair_recv.at[way, step, slot],
            self.place.sibling(),
        )

    def own_pair(self):
        held = self.shard(self.place.sp, None)
        return remote(
            held,
            held,
            self.edge.at[0],
            self.edge.at[1],
            self.place.sibling(),
        )

    def give(self, half, source):
        return remote(
            source,
            self.shard(self.place.sp, half),
            self.edge.at[2 + half],
            self.edge.at[4],
            self.place.along_y(half),
        )

    def taken(self):
        held = self.shard(2 * self.place.z + 1 - self.place.y, self.place.c)
        return remote(held, held, self.edge.at[2], self.edge.at[4], self.place.along_y(0))

    def pass_on(self, step, slot):
        for way in range(2):

            @pl.when(self.place.passes(way))
            def _(way=way):
                self.hop(way, step, slot).start()

    def share_own(self):
        @pl.when(self.place.home)
        def _():
            self.own_pair().start()

        @pl.when(jnp.logical_not(self.place.home))
        def _():
            self.own_pair().wait_recv()

    def share_taken(self):
        self.taken().wait_recv()
        held = self.shard(2 * self.place.z + 1 - self.place.y, self.place.c)
        self.other_pair(held).start()

    def other_pair(self, held):
        return remote(
            held, held, self.edge.at[5], self.edge.at[6], self.place.sibling()
        )

    def taken_pair(self):
        return self.other_pair(
            self.shard(2 * self.place.z + 1 - self.place.y, self.place.c)
        )

    def advance(self):
        step, slot = self.events[self.done]
        self.done += 1
        if step == 0:
            if self.own_first:
                if slot == 0:
                    self.share_own()
                else:
                    self.share_taken()
            if self.place.planes > 1:
                self.pass_on(0, slot)
            return
        for way in range(2):

            @pl.when(self.place.has(way, step))
            def _(way=way):
                self.hop(way, step - 1, slot).wait_recv()
                self.pair(way, step, slot).start()
                if step + 1 < self.place.planes:

                    @pl.when(self.place.passes(way))
                    def _():
                        self.hop(way, step, slot).start()

    def upto(self, event):
        while self.done <= min(event, len(self.events) - 1):
            self.advance()

    def complete(self, step, slot):
        if (step, slot) in self.whole:
            return
        self.whole.add((step, slot))
        if step == 0:
            if slot == 1:
                self.taken_pair().wait_recv()
            return
        for way in range(2):

            @pl.when(self.place.has(way, step))
            def _(way=way):
                self.pair(way, step, slot).wait_recv()

    def sent_edges(self, gave):
        @pl.when(self.place.home)
        def _():
            self.own_pair().wait_send()

        @pl.when(jnp.logical_not(self.place.home))
        def _():
            for half in range(2):
                gave(half).wait_send()

        self.taken_pair().wait_send()

    def sent(self, event):
        step, slot = self.events[event]
        place = self.place
        for way in range(2):
            if step > 0:

                @pl.when(place.has(way, step))
                def _(way=way):
                    self.pair(way, step, slot).wait_send()

            if step + 1 < place.planes:

                @pl.when(place.has(way, step) & place.passes(way))
                def _(way=way):
                    self.hop(way, step, slot).wait_send()


def layer_kernel(
    count,
    tokens,
    w_pool_in,
    w_query,
    w_key_t,
    w_value_t,
    pool_map,
    w_out,
    gain_in,
    pool_scale_in,
    q_gain_in,
    k_gain_in,
    sinks_in,
    out,
    normed,
    first_weights,
    last_weights,
    own_shard,
    acc,
    queries,
    keys_low,
    keys_high,
    values_low,
    values_high,
    pool_span,
    pairs,
    mixed,
    bias,
    band,
    ones_block,
    halo_pairs,
    halo_pool,
    from_x,
    from_pair,
    from_away,
    from_last,
    key_value,
    pool_maps,
    gain,
    pool_scales,
    q_gain,
    k_gain,
    sinks,
    head_rows,
    local_sem,
    first_sems,
    last_sems,
    first_edge,
    last_edge,
    near_sem,
    far_sem,
    send_sem,
    relay_sem,
    table_sem,
    halo_sem,
    sum_send,
    sum_recv,
):
    place = Place(count)
    x, y, z, c = place.x, place.y, place.z, place.c
    home, away = place.home, jnp.logical_not(place.home)
    me, seq = place.group, place.rows_of
    rows, width = tokens.shape
    depth, branch = w_pool_in.shape
    head_columns = w_query.shape[1]
    mid = branch + head_columns
    piece = rows // TOKEN_CHUNKS
    blocks = rows // WINDOW
    out_rows = out.shape[0]
    out_width = w_out.shape[1]
    mix = w_out.shape[0]
    pairs_of_heads = head_columns // LANES

    barrier = pltpu.get_barrier_semaphore()

    def greet(device):
        pl.semaphore_signal(
            barrier, inc=1, device_id=device, device_id_type=pl.DeviceIdType.MESH
        )

    for way in range(2):

        @pl.when(place.passes(way))
        def _(way=way):
            greet(place.along_z(way))

    for core in range(2):
        greet(place.along_x(core))
        greet(place.along_y(core))
    greet(place.sibling())
    greetings = 5 + jnp.where(place.passes(0), 1, 0) + jnp.where(place.passes(1), 1, 0)

    def first_shard(owner, half):
        if half is None:
            return first_weights.at[aligned(owner, depth)]
        size = depth // 2
        return first_weights.at[pl.ds(pl.multiple_of(owner * depth + half * size, size), size)]

    def last_shard(owner, half):
        if half is None:
            return last_weights.at[owner]
        return last_weights.at[owner, aligned(half, mix // 2)]

    first = Chain(
        place, first_shard, True, [first_sems.at[i] for i in range(4)] + [first_edge]
    )
    last = Chain(place, last_shard, False, [last_sems.at[i] for i in range(4)] + [last_edge])

    def local_copy(index, source, target):
        return pltpu.make_async_copy(source, target, local_sem.at[index])

    own_rows = aligned(place.sp, depth)
    small = [
        local_copy(0, w_key_t, key_value.at[pl.ds(0, HEAD_DIM)]),
        local_copy(1, w_value_t, key_value.at[pl.ds(HEAD_DIM, HEAD_DIM)]),
        local_copy(2, gain_in, gain),
        local_copy(3, q_gain_in, q_gain),
        local_copy(4, k_gain_in, k_gain),
    ]

    def shard_copies(target):
        return [
            local_copy(5, w_pool_in, target.at[:, pl.ds(0, branch)]),
            local_copy(6, w_query, target.at[:, pl.ds(branch, head_columns)]),
        ]

    def home_copies():
        return [
            local_copy(7, tokens, normed.at[:, aligned(place.tp, width)]),
            local_copy(8, w_out, last_weights.at[place.sp]),
            local_copy(9, pool_map, pool_maps),
            local_copy(10, pool_scale_in, pool_scales),
            local_copy(11, sinks_in, sinks),
        ]

    for copy in small[:2]:
        copy.start()

    @pl.when(home)
    def _():
        for copy in shard_copies(first_weights.at[own_rows]) + home_copies():
            copy.start()

    @pl.when(away)
    def _():
        for copy in shard_copies(own_shard):
            copy.start()

    for copy in small[2:]:
        copy.start()
    small[0].wait()
    small[1].wait()
    pair_columns = key_value[...].astype(f32).T.astype(bf16)

    def table_copies():
        return [
            remote(
                source,
                target,
                table_sem.at[0, index],
                table_sem.at[1, index],
                place.sibling(),
            )
            for index, (source, target) in enumerate(
                [(pool_map, pool_maps), (pool_scale_in, pool_scales), (sinks_in, sinks)]
            )
        ]

    def first_gave(half):
        return first.give(half, own_shard.at[pl.ds(half * (depth // 2), depth // 2)])

    def last_gave(half):
        return last.give(half, w_out.at[pl.ds(half * (mix // 2), mix // 2)])

    @pl.when(home)
    def _():
        first_weights[own_rows, pl.ds(mid, LANES)] = pair_columns
        for copy in shard_copies(first_weights.at[own_rows]):
            copy.wait()

    @pl.when(away)
    def _():
        own_shard[:, pl.ds(mid, LANES)] = pair_columns
        for copy in shard_copies(own_shard):
            copy.wait()

    pl.semaphore_wait(barrier, greetings)

    @pl.when(away)
    def _():
        for half in range(2):
            first_gave(half).start()

    def token_rows(chunk):
        return pl.ds(chunk * piece, piece)

    def landing(chunk, side, core):
        owner = 2 * (jnp.where(x == 0, side, 1 - side)) + core
        return normed.at[token_rows(chunk), aligned(owner, width)]

    def to_sibling(chunk):
        return remote(
            tokens.at[token_rows(chunk)],
            landing(chunk, 0, c),
            send_sem.at[0, chunk],
            near_sem.at[c, chunk],
            place.sibling(),
        )

    def to_x(chunk):
        return remote(
            tokens.at[token_rows(chunk)],
            landing(chunk, 0, c),
            send_sem.at[1, chunk],
            far_sem.at[c, chunk],
            place.along_x(y),
        )

    def to_y(chunk):
        return remote(
            tokens.at[token_rows(chunk)],
            landing(chunk, 0, c),
            send_sem.at[2, chunk],
            near_sem.at[c, chunk],
            place.along_y(y),
        )

    def by_x(chunk, core):
        return core == 1 or chunk == 1

    def relay(chunk, core):
        if by_x(chunk, core):
            held = landing(chunk, 0, core)
            device = place.along_x(c)
        else:
            held = landing(chunk, 1, core)
            device = place.along_y(c)
        return remote(
            held, held, relay_sem.at[core, chunk], far_sem.at[core, chunk], device
        )

    def near_wait(chunk, core):
        held = landing(chunk, 0, core)
        remote(
            held, held, send_sem.at[0, chunk], near_sem.at[core, chunk], place.sibling()
        ).wait_recv()

    def far_wait(chunk, core):
        held = landing(chunk, 1, core)
        remote(
            held, held, send_sem.at[0, chunk], far_sem.at[core, chunk], place.sibling()
        ).wait_recv()

    ahead = 3

    def send_tokens(chunk):
        to_x(chunk).start()
        to_y(chunk).start()

    @pl.when(home)
    def _():
        for copy in table_copies():
            copy.start()

    first.upto(0)
    for chunk in range(ahead):
        to_x(chunk).start()

    @pl.when(away)
    def _():
        for chunk in range(TOKEN_CHUNKS):
            to_sibling(chunk).start()
        for chunk in range(ahead):
            to_y(chunk).start()

    span = 2.0 * jnp.exp2(me.astype(f32))
    row = lax.broadcasted_iota(jnp.int32, (WINDOW, 2 * WINDOW), 0)
    column = lax.broadcasted_iota(jnp.int32, (WINDOW, 2 * WINDOW), 1)
    distance = (row + WINDOW - column).astype(f32)
    band[...] = jnp.where((distance >= 0.0) & (distance < span), 1.0, 0.0).astype(bf16)
    allowed = (distance >= 0.0) & (distance < float(WINDOW))
    for pair in range(pairs_of_heads):
        for half in range(2):
            head = (me * GROUP + 2 * pair + half + 1).astype(f32)
            slope = jnp.exp2(jnp.full((WINDOW, 2 * WINDOW), -8.0 / Q_HEADS, f32) * head)
            bias[pl.ds(pair * WINDOW, WINDOW), pl.ds(half * 2 * WINDOW, 2 * WINDOW)] = jnp.where(
                allowed, -slope * distance, MASKED
            )
    block_row = lax.broadcasted_iota(jnp.int32, (2 * LANES, 2 * LANES), 0) // HEAD_DIM
    block_column = lax.broadcasted_iota(jnp.int32, (2 * LANES, 2 * LANES), 1) // HEAD_DIM
    ones_block[...] = jnp.where(block_row == block_column, 1.0, 0.0).astype(bf16)
    pool_span[pl.ds(0, WINDOW)] = jnp.zeros((WINDOW, branch), bf16)

    acc[...] = jnp.zeros(acc.shape, f32)
    strip = 32

    def normalise(chunk):
        @pl.loop(0, piece // strip)
        def _(index):
            held = pl.ds(pl.multiple_of(chunk * piece + index * strip, strip), strip)
            values = normed[held].astype(f32)
            scale = lax.rsqrt(jnp.mean(values * values, axis=-1, keepdims=True) + epsilon)
            normed[held] = (values * scale * gain[...]).astype(bf16)

    lane = lax.broadcasted_iota(jnp.int32, (1, LANES), 1)
    low = lane < HEAD_DIM
    for copy in small[2:]:
        copy.wait()

    @pl.when(home)
    def _():
        for copy in home_copies():
            copy.wait()
        last.own_pair().start()

    @pl.when(away)
    def _():
        for copy in table_copies():
            copy.wait_recv()

    head_rows[...] = jnp.zeros(head_rows.shape, f32)
    head_rows[pl.ds(0, 1), pl.ds(0, HEAD_DIM)] = q_gain[...] * HEAD_DIM**-0.5
    head_rows[pl.ds(1, 1), pl.ds(0, HEAD_DIM)] = k_gain[...]
    once = head_rows[pl.ds(0, 1), :]
    head_rows[pl.ds(0, 1), :] = once + pltpu.roll(once, HEAD_DIM, 1)
    for pair in range(pairs_of_heads):
        one, two = sinks[:, 2 * pair : 2 * pair + 1], sinks[:, 2 * pair + 1 : 2 * pair + 2]
        head_rows[pl.ds(2 + pair, 1), :] = jnp.exp(
            jnp.where(low, jnp.broadcast_to(one, (1, LANES)), jnp.broadcast_to(two, (1, LANES)))
        )

    tile = piece

    def multiply(chunks, steps):
        @pl.loop(steps[0], steps[1])
        def _(step):
            for way in range(2):

                @pl.when(place.has(way, step) & (step + way > 0))
                def _(way=way):
                    block = aligned(place.source(way, step), 2 * depth)

                    @pl.loop(chunks[0], chunks[1])
                    def _(index):
                        held = aligned(index, tile)
                        acc[held] += dot(normed[held, block], first_weights[block, :])

    class Progress:
        rows, steps = 0, 0

    def catch_up(chunks, steps):
        if steps > Progress.steps:
            for step in range(Progress.steps, steps):
                for slot in range(2):
                    first.complete(step, slot)
            if Progress.rows > 0:
                multiply((0, Progress.rows), (Progress.steps, steps))
            Progress.steps = steps
        if chunks > Progress.rows:
            if steps > 0:
                multiply((Progress.rows, chunks), (0, steps))
            Progress.rows = chunks

    def settle(chunk):
        for core in range(2):

            @pl.when(away if by_x(chunk, core) else home)
            def _(core=core):
                relay(chunk, core).wait_send()

        normalise(chunk)

    first.upto(1)
    first.complete(0, 1)

    @pl.when(home)
    def _():
        for chunk in range(ahead):
            to_y(chunk).start()

    events = len(first.events)

    def pass_tokens(chunk):
        @pl.when(home)
        def _():
            for core in range(2):
                far_wait(chunk, core)
                if not by_x(chunk, core):
                    relay(chunk, core).start()
            near_wait(chunk, 1 - c)

        @pl.when(away)
        def _():
            for core in range(2):
                near_wait(chunk, core)
                if by_x(chunk, core):
                    relay(chunk, core).start()

        if chunk + ahead < TOKEN_CHUNKS:
            send_tokens(chunk + ahead)

    def use_tokens(chunk):
        @pl.when(away)
        def _():
            for core in range(2):
                far_wait(chunk, core)
            if chunk == TOKEN_CHUNKS - 1:
                for half in range(2):
                    last_gave(half).start()

        settle(chunk)
        catch_up(chunk + 1, first.done // 2)

    for chunk in range(TOKEN_CHUNKS):
        first.upto((chunk + 3) * events // 8 - 1)
        pass_tokens(chunk)
        if chunk > 1:
            use_tokens(chunk - 2)

    @pl.when(away)
    def _():
        last.own_pair().wait_recv()

    first.upto(7 * events // 8 - 1)
    last.pass_on(0, y)
    for chunk in range(max(0, TOKEN_CHUNKS - 2), TOKEN_CHUNKS):
        use_tokens(chunk)
    first.upto(events - 1)
    catch_up(TOKEN_CHUNKS, place.planes)

    one_low = jnp.where(low, 1.0, 0.0)

    def spread(kv, held, count_scale):
        size = kv.shape[0]
        key_low = jnp.where(low, kv, 0.0)
        value_high = jnp.where(low, 0.0, kv)
        keys_low[held] = key_low.astype(bf16)
        keys_high[held] = pltpu.roll(key_low, HEAD_DIM, 1).astype(bf16)
        ones_low = jnp.broadcast_to(one_low * count_scale, (size, LANES)).astype(bf16)
        ones_high = jnp.broadcast_to((1.0 - one_low) * count_scale, (size, LANES)).astype(bf16)
        values_low[held, pl.ds(0, LANES)] = pltpu.roll(value_high, HEAD_DIM, 1).astype(bf16)
        values_low[held, pl.ds(LANES, LANES)] = ones_low
        values_high[held, pl.ds(0, LANES)] = value_high.astype(bf16)
        values_high[held, pl.ds(LANES, LANES)] = ones_high

    def finalise(index):
        held = aligned(index, tile)
        sums = acc[held].astype(bf16)
        shifted = pl.ds(pl.multiple_of(index * tile + WINDOW, WINDOW), tile)
        pool_span[shifted] = sums[:, :branch]
        kv = sums[:, mid:].astype(f32)
        squares = jnp.where(low, kv * kv, 0.0)
        scale = lax.rsqrt(jnp.sum(squares, axis=-1, keepdims=True) * (1.0 / HEAD_DIM) + epsilon)
        kv = jnp.where(low, kv * scale * head_rows[pl.ds(1, 1), :], kv).astype(bf16)
        pairs[held] = kv
        spread(kv.astype(f32), shifted, 1.0)
        wide = 2 * LANES
        gain_row = head_rows[pl.ds(0, 1), :]
        query_gain = jnp.concatenate([gain_row, gain_row], axis=1)
        for start in range(0, head_columns, wide):
            query = sums[:, branch + start : branch + start + wide].astype(f32)
            square = query * query
            upper = square.astype(bf16)
            lower = (square - upper.astype(f32)).astype(bf16)
            total = dot(upper, ones_block[...]) + dot(lower, ones_block[...])
            scale = lax.rsqrt(total * (1.0 / HEAD_DIM) + epsilon)
            queries[held, pl.ds(start, wide)] = (
                query * scale * query_gain
            ).astype(bf16)

    def halo_copies(device):
        return [
            remote(
                source,
                target,
                halo_sem.at[0, index],
                halo_sem.at[1, index],
                device,
            )
            for index, (source, target) in enumerate(
                [
                    (pairs.at[pl.ds(rows - WINDOW, WINDOW)], halo_pairs),
                    (pool_span.at[pl.ds(WINDOW + rows - HALO_ROWS, HALO_ROWS)], halo_pool),
                ]
            )
        ]

    next_plane = {"sp": place.sp + 2, "tp": 2 * x}
    sends_up = (c == 1) & place.passes(0)
    finalise(rows // tile - 1)

    @pl.when(c == 0)
    def _():
        for copy in halo_copies({"tp": 2 * x + 1}):
            copy.start()

    @pl.when(sends_up)
    def _():
        for copy in halo_copies(next_plane):
            copy.start()

    @pl.loop(0, rows // tile - 1)
    def _(index):
        finalise(index)

    def pool(block):
        held = aligned(block, WINDOW)
        span_rows = pool_span[pl.ds(pl.multiple_of(block * WINDOW, WINDOW), 2 * WINDOW)]
        running = dot(band[...], span_rows)
        offset = lax.broadcasted_iota(jnp.int32, (WINDOW, 1), 0)
        position = (seq * rows + block * WINDOW + offset).astype(f32)
        counted = jnp.minimum(position + 1.0, span)
        difference = (running / counted - span_rows[WINDOW:].astype(f32)).astype(bf16)
        mapped = dot(difference, pool_maps[...]) * pool_scales[...]
        scale = lax.rsqrt(jnp.mean(mapped * mapped, axis=-1, keepdims=True) + epsilon)
        mixed[held, pl.ds(0, branch)] = (mapped * scale).astype(bf16)

    def attend(block):
        held = aligned(block, WINDOW)
        both = pl.ds(pl.multiple_of(block * WINDOW, WINDOW), 2 * WINDOW)
        key_pair = jnp.concatenate([keys_low[both], keys_high[both]], axis=0)
        value_pair = jnp.concatenate([values_low[both], values_high[both]], axis=0)
        parts, squares = [], None
        for pair in range(pairs_of_heads):
            lanes = pl.ds(pair * LANES, LANES)
            scores = lax.dot_general(
                queries[held, lanes],
                key_pair,
                (((1,), (1,)), ((), ())),
                preferred_element_type=f32,
            )
            weights = jnp.exp(scores + bias[pl.ds(pair * WINDOW, WINDOW)]).astype(bf16)
            result = dot(weights, value_pair)
            part = result[:, :LANES] / (
                result[:, LANES:] + head_rows[pl.ds(2 + pair, 1), :]
            )
            parts.append(part)
            squares = part * part if squares is None else squares + part * part
        mean = jnp.sum(squares, axis=-1, keepdims=True) * (1.0 / head_columns)
        scale = lax.rsqrt(mean + epsilon)
        for pair, part in enumerate(parts):
            mixed[held, pl.ds(branch + pair * LANES, LANES)] = (part * scale).astype(bf16)

    half = (blocks + 1) // 2

    @pl.loop(1, half + 1)
    def _(block):
        pool(block)
        attend(block)

    last.share_taken()
    last.pass_on(0, 1 - y)
    last.done = 2

    @pl.loop(half + 1, blocks)
    def _(block):
        pool(block)
        attend(block)

    begun = jnp.where(seq > 0, 1.0, 0.0)
    top = pl.ds(0, WINDOW)

    @pl.when(seq > 0)
    def _():
        for copy in halo_copies(next_plane):
            copy.wait_recv()
        spread(halo_pairs[...].astype(f32), top, 1.0)
        pool_span[pl.ds(WINDOW - HALO_ROWS, HALO_ROWS)] = halo_pool[...]

    @pl.when(seq == 0)
    def _():
        for ref in (keys_low, keys_high, values_low, values_high):
            ref[top] = jnp.zeros((WINDOW, ref.shape[1]), bf16)

    pool(0)
    attend(0)

    if out_width % (2 * LANES) == 0:
        units_of = {0: [(1, 0), (2, out_width // 2)], 1: [(1, 0), (2, out_width // 2)]}
        unit_width = out_width // 2
    else:
        units_of = {0: [(1, 0)], 1: [(2, 0)]}
        unit_width = out_width

    step_of = min(unit_width, LANES)

    class Shard:
        def __init__(self, owner, slot):
            self.owner, self.units = owner, units_of[slot]

        def lanes(self, start, size):
            return pl.ds(pl.multiple_of(self.owner * out_width + start, step_of), size)

        def unit(self, start):
            return self.lanes(start, unit_width)

        def packed(self):
            index = self.owner if len(self.units) == 2 else self.owner // 2
            return aligned(index, unit_width)

        def copy(self, source, target, sent, landed, device):
            return remote(
                source,
                target,
                sum_send.at[sent, self.owner],
                sum_recv.at[landed, self.owner],
                device,
            )

        def row_block(self, index, lanes):
            return normed.at[aligned(index, out_rows), lanes]

        def across_x(self, start):
            lanes = self.unit(start)
            return self.copy(
                normed.at[aligned(1 - x, 2 * out_rows), lanes],
                from_x.at[:, self.packed()],
                0,
                0,
                place.along_x(c),
            )

        def across_y(self, start):
            return self.copy(
                normed.at[:, self.unit(start)],
                from_away.at[:, self.packed()],
                1,
                1,
                place.along_y(c),
            )

        def to_pair(self):
            lanes = self.lanes(0, out_width)
            return self.copy(
                self.row_block(2 * x + 1 - c, lanes),
                from_pair.at[:, lanes],
                1,
                1,
                place.sibling(),
            )

        def away_final(self, start, core):
            lanes = self.unit(start)
            return self.copy(
                self.row_block(2 * x + core, lanes),
                from_last.at[:, lanes],
                2 + core,
                2,
                place.along_y(core),
            )

        def home_final(self, start, core):
            lanes = self.unit(start)
            return self.copy(
                self.row_block(2 * (1 - x) + core, lanes),
                from_last.at[:, lanes],
                4 + core,
                3,
                place.along_x(core),
            )

        def first(self):
            lanes = self.lanes(0, out_width)

            @pl.loop(0, 4)
            def _(index):
                held = aligned((2 * (1 - x) + index) % 4, out_rows)
                normed[held, lanes] = dot(mixed[held, :], last_weights[self.owner]).astype(bf16)

            for scheme, start in self.units:
                if scheme == 1:
                    self.across_x(start).start()
                else:

                    @pl.when(away)
                    def _(start=start):
                        self.across_y(start).start()

        def second(self):
            for scheme, start in self.units:
                lanes = self.unit(start)
                if scheme == 1:
                    self.across_x(start).wait_recv()
                    held = aligned(x, 2 * out_rows)
                    normed[held, lanes] = (
                        normed[held, lanes].astype(f32) + from_x[:, self.packed()].astype(f32)
                    ).astype(bf16)

                    @pl.when(away)
                    def _(start=start):
                        for core in range(2):
                            self.away_final(start, core).start()
                else:

                    @pl.when(home)
                    def _(start=start, lanes=lanes):
                        self.across_y(start).wait_recv()

                        @pl.loop(0, 4)
                        def _(index):
                            held = aligned(index, out_rows)
                            normed[held, lanes] = (
                                normed[held, lanes].astype(f32)
                                + from_away[held, self.packed()].astype(f32)
                            ).astype(bf16)

                        for core in range(2):
                            self.home_final(start, core).start()

            @pl.when(home)
            def _():
                self.to_pair().start()

        def third(self):
            lanes = self.lanes(0, out_width)
            for scheme, start in self.units:
                if scheme == 1:
                    self.away_final(start, 0).wait_recv()
                else:
                    self.home_final(start, 0).wait_recv()

            @pl.when(home)
            def _():
                out[:, lanes] = (
                    normed[aligned(2 * x + c, out_rows), lanes].astype(f32)
                    + from_last[:, lanes].astype(f32)
                ).astype(bf16)

            @pl.when(away)
            def _():
                self.to_pair().wait_recv()
                out[:, lanes] = (
                    from_pair[:, lanes].astype(f32) + from_last[:, lanes].astype(f32)
                ).astype(bf16)

        def sent(self):
            for scheme, start in self.units:
                if scheme == 1:
                    self.across_x(start).wait_send()

                    @pl.when(away)
                    def _(start=start):
                        for core in range(2):
                            self.away_final(start, core).wait_send()
                else:

                    @pl.when(away)
                    def _(start=start):
                        self.across_y(start).wait_send()

                    @pl.when(home)
                    def _(start=start):
                        for core in range(2):
                            self.home_final(start, core).wait_send()

            @pl.when(home)
            def _():
                self.to_pair().wait_send()

    def each(event, stage):
        step, slot = last.events[event]

        @pl.loop(0, 1 if step == 0 else 2)
        def _(way):
            plane = z + (2 * way - 1) * step

            @pl.when((plane >= 0) & (plane < place.planes))
            def _():
                getattr(Shard(2 * plane + slot, slot), stage)()

    last.taken_pair().wait_recv()
    total = len(last.events)

    def early_sends():
        for chunk in range(TOKEN_CHUNKS):
            to_x(chunk).wait_send()
            to_y(chunk).wait_send()

        @pl.when(away)
        def _():
            for chunk in range(TOKEN_CHUNKS):
                to_sibling(chunk).wait_send()

        @pl.when(home)
        def _():
            for copy in table_copies():
                copy.wait_send()

        @pl.when((c == 0) | sends_up)
        def _():
            for copy in halo_copies(next_plane):
                copy.wait_send()

        first.sent_edges(first_gave)
        last.sent_edges(last_gave)
        for event in range(total):
            first.sent(event)

    for event, (step, slot) in enumerate(last.events):
        last.upto(event)
        if step > 0:
            last.complete(step, slot)
        each(event, "first")
        if event > 0:
            each(event - 1, "second")
        if event > 2:
            each(event - 3, "third")
        if event == min(3, total - 1):
            early_sends()
        if event > 3:
            last.sent(event - 4)
            each(event - 4, "sent")
    each(total - 1, "second")
    for event in range(max(0, total - 3), total):
        each(event, "third")
    for event in range(max(0, total - 4), total):
        last.sent(event)
        each(event, "sent")


def layer(tokens, w_pool_in, w_query, w_key_t, w_value_t, pool_map, w_out, *rows_in):
    count = lax.axis_size("sp")
    rows, width = tokens.shape
    depth, branch = w_pool_in.shape
    head_columns = w_query.shape[1]
    features = width * lax.axis_size("tp")
    mix, out_width = w_out.shape
    out_rows = rows // lax.axis_size("tp")
    out_columns = count * out_width
    sums = branch + head_columns + LANES
    dma = pltpu.SemaphoreType.DMA
    planes = count // 2
    hbm = pl.BlockSpec(memory_space=pltpu.HBM)
    flops = 2 * rows * features * sums + 2 * rows * mix * out_columns
    return pl.pallas_call(
        functools.partial(layer_kernel, count),
        out_shape=pltpu.VMEM((out_rows, out_columns), bf16),
        in_specs=[hbm] * 12,
        out_specs=pl.BlockSpec(memory_space=pltpu.VMEM),
        scratch_shapes=[
            pltpu.VMEM((rows, features), bf16),
            pltpu.VMEM((features, sums), bf16),
            pltpu.VMEM((count, mix, out_width), bf16),
            pltpu.VMEM((depth, sums), bf16),
            pltpu.VMEM((rows, sums), f32),
            pltpu.VMEM((rows, head_columns), bf16),
            pltpu.VMEM((WINDOW + rows, LANES), bf16),
            pltpu.VMEM((WINDOW + rows, LANES), bf16),
            pltpu.VMEM((WINDOW + rows, 2 * LANES), bf16),
            pltpu.VMEM((WINDOW + rows, 2 * LANES), bf16),
            pltpu.VMEM((WINDOW + rows, branch), bf16),
            pltpu.VMEM((rows, LANES), bf16),
            pltpu.VMEM((rows, mix), bf16),
            pltpu.VMEM((head_columns // LANES * WINDOW, 4 * WINDOW), f32),
            pltpu.VMEM((WINDOW, 2 * WINDOW), bf16),
            pltpu.VMEM((2 * LANES, 2 * LANES), bf16),
            pltpu.VMEM((WINDOW, LANES), bf16),
            pltpu.VMEM((HALO_ROWS, branch), bf16),
            pltpu.VMEM((2 * out_rows, out_columns // 2), bf16),
            pltpu.VMEM((out_rows, out_columns), bf16),
            pltpu.VMEM((rows, out_columns // 2), bf16),
            pltpu.VMEM((out_rows, out_columns), bf16),
            pltpu.VMEM((2 * HEAD_DIM, depth), bf16),
            pltpu.VMEM((branch, branch), bf16),
            pltpu.VMEM((1, features), f32),
            pltpu.VMEM((1, branch), f32),
            pltpu.VMEM((1, HEAD_DIM), f32),
            pltpu.VMEM((1, HEAD_DIM), f32),
            pltpu.VMEM((1, GROUP), f32),
            pltpu.VMEM((8, LANES), f32),
            dma((12,)),
            dma((4, 2, planes, 2)),
            dma((4, 2, planes, 2)),
            dma((7,)),
            dma((7,)),
            dma((2, TOKEN_CHUNKS)),
            dma((2, TOKEN_CHUNKS)),
            dma((3, TOKEN_CHUNKS)),
            dma((2, TOKEN_CHUNKS)),
            dma((2, 3)),
            dma((2, 2)),
            dma((6, count)),
            dma((4, count)),
        ],
        compiler_params=pltpu.CompilerParams(
            collective_id=0, has_side_effects=True, vmem_limit_bytes=60 * 1024 * 1024
        ),
        cost_estimate=pl.CostEstimate(
            flops=flops, bytes_accessed=4 * rows * width, transcendentals=0
        ),
    )(tokens, w_pool_in, w_query, w_key_t, w_value_t, pool_map, w_out, *rows_in)


def local(
    tokens,
    norm_gain,
    w_pool_in,
    w_query,
    w_key,
    w_value,
    pool_map,
    pool_scale,
    q_gain,
    k_gain,
    sinks,
    w_out,
):
    return layer(
        tokens,
        w_pool_in,
        w_query,
        w_key.T,
        w_value.T,
        pool_map[0],
        w_out,
        norm_gain[None],
        pool_scale[None],
        q_gain[None],
        k_gain[None],
        sinks[None],
    )


def solution(mesh):
    in_specs = (
        P("sp", "tp"),
        P(),
        P("sp", "tp"),
        P("sp", "tp"),
        P("sp", "tp"),
        P("sp", "tp"),
        P("tp", None, None),
        P("tp"),
        P(),
        P(),
        P("tp"),
        P("tp", "sp"),
    )
    out_specs = P(("sp", "tp"), None)
    return jax.shard_map(local, mesh=mesh, in_specs=in_specs, out_specs=out_specs, check_vma=False)
```

time: 185 us -> 175 us (0.946)
  Pallas kernels: 183 us -> 174 us
    pallas_call x1, Pallas kernels: 183 us -> 174 us  [layer(): pl.pallas_call(functools.partial(layer_kernel, count), out_shape=pltpu.VM...]
where the time goes in v3:
time: 175 us
  Pallas kernels  174 us (99%)
    pallas_call x1, Pallas kernels, layer(): pl.pallas_call(functools.partial(layer_kernel, count), out_shape=pltpu.VM...  174 us

profile of v3, /device:TPU:1, one launch (start us, length us, event | category | flops | bytes accessed | tf_op | source)
XLA Modules:
  0.0 174.8 jit_solution(12371487840637589771)
XLA Ops:
  0.0 173.5 %shard_map.118 = bf16[256,4096]{1,0:T(8,128)(2,1)S(1)} custom-call(bf16[1024,1024]{1,0:T(8,128)(2,1)} %tokens.1, bf16[512,512]{1,0:T(8,128)(2,1)} %w_pool_in.1, bf16[512,512]{1,0:T(8,128)(2,1)} %w_query.1, bf16[64,512]{1,0:T(8,128)(2,1)} %bitcast.9, bf16[64,512]{1,0:T(8,128)(2,1)} %bitcast.10, bf16[512,512]{1,0:T(8,128)(2,1)} %bitcast.8, ...), custom_call_target="tpu_custom_call" | custom-call | flops 18253611008 | bytes 4194304 | tf_op jit(solution)/shard_map/pallas_call | solution.py:1064
  173.5 1.3 copy.14

commit v4 on v3

--- a/solution.py
+++ b/solution.py
@@ -73,7 +73,7 @@
 class Chain:
     def __init__(self, place, shard, own_first, sems):
         self.place, self.shard, self.own_first = place, shard, own_first
-        self.up_send, self.up_recv, self.pair_send, self.pair_recv, self.edge = sems
+        self.up_send, self.up_recv, self.pair_recv, self.edge = sems
         self.events = [(step, slot) for step in range(place.planes) for slot in range(2)]
         self.done, self.whole = 0, set()
 
@@ -96,8 +96,8 @@
         return remote(
             held,
             held,
-            self.pair_send.at[way, step, slot],
-            self.pair_recv.at[way, step, slot],
+            self.edge.at[7],
+            self.pair_recv.at[way, step - 1, slot],
             self.place.sibling(),
         )
 
@@ -212,18 +212,17 @@
     def sent(self, event):
         step, slot = self.events[event]
         place = self.place
-        for way in range(2):
-            if step > 0:
-
-                @pl.when(place.has(way, step))
-                def _(way=way):
-                    self.pair(way, step, slot).wait_send()
-
-            if step + 1 < place.planes:
+        if step + 1 < place.planes:
+            for way in range(2):
 
                 @pl.when(place.has(way, step) & place.passes(way))
                 def _(way=way):
                     self.hop(way, step, slot).wait_send()
+
+    def shared(self, whole):
+        remote(
+            whole, whole, self.edge.at[7], self.edge.at[0], self.place.sibling()
+        ).wait_send()
 
 
 def layer_kernel(
@@ -284,6 +283,7 @@
     halo_sem,
     sum_send,
     sum_recv,
+    half_recv,
 ):
     place = Place(count)
     x, y, z, c = place.x, place.y, place.z, place.c
@@ -331,9 +331,9 @@
         return last_weights.at[owner, aligned(half, mix // 2)]
 
     first = Chain(
-        place, first_shard, True, [first_sems.at[i] for i in range(4)] + [first_edge]
+        place, first_shard, True, [first_sems.at[i] for i in range(3)] + [first_edge]
     )
-    last = Chain(place, last_shard, False, [last_sems.at[i] for i in range(4)] + [last_edge])
+    last = Chain(place, last_shard, False, [last_sems.at[i] for i in range(3)] + [last_edge])
 
     def local_copy(index, source, target):
         return pltpu.make_async_copy(source, target, local_sem.at[index])
@@ -431,7 +431,7 @@
         return remote(
             tokens.at[token_rows(chunk)],
             landing(chunk, 0, c),
-            send_sem.at[0, chunk],
+            send_sem.at[0],
             near_sem.at[c, chunk],
             place.sibling(),
         )
@@ -440,7 +440,7 @@
         return remote(
             tokens.at[token_rows(chunk)],
             landing(chunk, 0, c),
-            send_sem.at[1, chunk],
+            send_sem.at[1],
             far_sem.at[c, chunk],
             place.along_x(y),
         )
@@ -449,7 +449,7 @@
         return remote(
             tokens.at[token_rows(chunk)],
             landing(chunk, 0, c),
-            send_sem.at[2, chunk],
+            send_sem.at[2],
             near_sem.at[c, chunk],
             place.along_y(y),
         )
@@ -471,13 +471,13 @@
     def near_wait(chunk, core):
         held = landing(chunk, 0, core)
         remote(
-            held, held, send_sem.at[0, chunk], near_sem.at[core, chunk], place.sibling()
+            held, held, send_sem.at[0], near_sem.at[core, chunk], place.sibling()
         ).wait_recv()
 
     def far_wait(chunk, core):
         held = landing(chunk, 1, core)
         remote(
-            held, held, send_sem.at[0, chunk], far_sem.at[core, chunk], place.sibling()
+            held, held, send_sem.at[0], far_sem.at[core, chunk], place.sibling()
         ).wait_recv()
 
     ahead = 3
@@ -638,7 +638,10 @@
                     last_gave(half).start()
 
         settle(chunk)
-        catch_up(chunk + 1, first.done // 2)
+        known = first.done // 2
+        if chunk == TOKEN_CHUNKS - 1:
+            first.upto(events - 1)
+        catch_up(chunk + 1, known)
 
     for chunk in range(TOKEN_CHUNKS):
         first.upto((chunk + 3) * events // 8 - 1)
@@ -654,7 +657,6 @@
     last.pass_on(0, y)
     for chunk in range(max(0, TOKEN_CHUNKS - 2), TOKEN_CHUNKS):
         use_tokens(chunk)
-    first.upto(events - 1)
     catch_up(TOKEN_CHUNKS, place.planes)
 
     one_low = jnp.where(low, 1.0, 0.0)
@@ -770,40 +772,6 @@
         for pair, part in enumerate(parts):
             mixed[held, pl.ds(branch + pair * LANES, LANES)] = (part * scale).astype(bf16)
 
-    half = (blocks + 1) // 2
-
-    @pl.loop(1, half + 1)
-    def _(block):
-        pool(block)
-        attend(block)
-
-    last.share_taken()
-    last.pass_on(0, 1 - y)
-    last.done = 2
-
-    @pl.loop(half + 1, blocks)
-    def _(block):
-        pool(block)
-        attend(block)
-
-    begun = jnp.where(seq > 0, 1.0, 0.0)
-    top = pl.ds(0, WINDOW)
-
-    @pl.when(seq > 0)
-    def _():
-        for copy in halo_copies(next_plane):
-            copy.wait_recv()
-        spread(halo_pairs[...].astype(f32), top, 1.0)
-        pool_span[pl.ds(WINDOW - HALO_ROWS, HALO_ROWS)] = halo_pool[...]
-
-    @pl.when(seq == 0)
-    def _():
-        for ref in (keys_low, keys_high, values_low, values_high):
-            ref[top] = jnp.zeros((WINDOW, ref.shape[1]), bf16)
-
-    pool(0)
-    attend(0)
-
     if out_width % (2 * LANES) == 0:
         units_of = {0: [(1, 0), (2, out_width // 2)], 1: [(1, 0), (2, out_width // 2)]}
         unit_width = out_width // 2
@@ -814,8 +782,10 @@
     step_of = min(unit_width, LANES)
 
     class Shard:
-        def __init__(self, owner, slot):
-            self.owner, self.units = owner, units_of[slot]
+        def __init__(self, owner, event):
+            slot = last.events[event][1]
+            self.owner, self.event = owner, event
+            self.units = units_of[slot]
 
         def lanes(self, start, size):
             return pl.ds(pl.multiple_of(self.owner * out_width + start, step_of), size)
@@ -824,37 +794,36 @@
             return self.lanes(start, unit_width)
 
         def packed(self):
-            index = self.owner if len(self.units) == 2 else self.owner // 2
-            return aligned(index, unit_width)
+            return aligned(self.owner if len(self.units) == 2 else self.owner // 2, unit_width)
 
         def copy(self, source, target, sent, landed, device):
             return remote(
-                source,
-                target,
-                sum_send.at[sent, self.owner],
-                sum_recv.at[landed, self.owner],
-                device,
+                source, target, sum_send.at[sent], sum_recv.at[landed, self.owner], device
             )
 
         def row_block(self, index, lanes):
             return normed.at[aligned(index, out_rows), lanes]
 
         def across_x(self, start):
-            lanes = self.unit(start)
             return self.copy(
-                normed.at[aligned(1 - x, 2 * out_rows), lanes],
+                normed.at[aligned(1 - x, 2 * out_rows), self.unit(start)],
                 from_x.at[:, self.packed()],
                 0,
                 0,
                 place.along_x(c),
             )
 
-        def across_y(self, start):
-            return self.copy(
-                normed.at[:, self.unit(start)],
-                from_away.at[:, self.packed()],
-                1,
-                1,
+        def across_y(self, start, part=None):
+            if part is None:
+                held = pl.ds(0, rows)
+            else:
+                held = aligned(1 - x if part == 0 else x, 2 * out_rows)
+            landed = half_recv.at[self.event] if part == 0 else sum_recv.at[1, self.owner]
+            return remote(
+                normed.at[held, self.unit(start)],
+                from_away.at[held, self.packed()],
+                sum_send.at[1],
+                landed,
                 place.along_y(c),
             )
 
@@ -883,27 +852,41 @@
             return self.copy(
                 self.row_block(2 * (1 - x) + core, lanes),
                 from_last.at[:, lanes],
-                4 + core,
+                2 + core,
                 3,
                 place.along_x(core),
             )
 
-        def first(self):
+        def terms(self, least, end):
             lanes = self.lanes(0, out_width)
 
-            @pl.loop(0, 4)
+            @pl.loop(least, end)
             def _(index):
                 held = aligned((2 * (1 - x) + index) % 4, out_rows)
                 normed[held, lanes] = dot(mixed[held, :], last_weights[self.owner]).astype(bf16)
 
+        def go_across(self, part):
             for scheme, start in self.units:
                 if scheme == 1:
-                    self.across_x(start).start()
+                    if part != 1:
+                        self.across_x(start).start()
                 else:
 
                     @pl.when(away)
-                    def _(start=start):
-                        self.across_y(start).start()
+                    def _():
+                        self.across_y(start, part).start()
+
+        def first(self):
+            self.terms(0, 4)
+            self.go_across(None)
+
+        def first_rows(self):
+            self.terms(0, 2)
+            self.go_across(0)
+
+        def other_rows(self):
+            self.terms(2, 4)
+            self.go_across(1)
 
         def second(self):
             for scheme, start in self.units:
@@ -916,14 +899,18 @@
                     ).astype(bf16)
 
                     @pl.when(away)
-                    def _(start=start):
+                    def _():
                         for core in range(2):
                             self.away_final(start, core).start()
                 else:
 
                     @pl.when(home)
-                    def _(start=start, lanes=lanes):
-                        self.across_y(start).wait_recv()
+                    def _():
+                        if self.event < 2:
+                            self.across_y(start, 0).wait_recv()
+                            self.across_y(start, 1).wait_recv()
+                        else:
+                            self.across_y(start).wait_recv()
 
                         @pl.loop(0, 4)
                         def _(index):
@@ -962,30 +949,6 @@
                     from_pair[:, lanes].astype(f32) + from_last[:, lanes].astype(f32)
                 ).astype(bf16)
 
-        def sent(self):
-            for scheme, start in self.units:
-                if scheme == 1:
-                    self.across_x(start).wait_send()
-
-                    @pl.when(away)
-                    def _(start=start):
-                        for core in range(2):
-                            self.away_final(start, core).wait_send()
-                else:
-
-                    @pl.when(away)
-                    def _(start=start):
-                        self.across_y(start).wait_send()
-
-                    @pl.when(home)
-                    def _(start=start):
-                        for core in range(2):
-                            self.home_final(start, core).wait_send()
-
-            @pl.when(home)
-            def _():
-                self.to_pair().wait_send()
-
     def each(event, stage):
         step, slot = last.events[event]
 
@@ -995,20 +958,67 @@
 
             @pl.when((plane >= 0) & (plane < place.planes))
             def _():
-                getattr(Shard(2 * plane + slot, slot), stage)()
-
+                getattr(Shard(2 * plane + slot, event), stage)()
+
+    def take_halo():
+        top = pl.ds(0, WINDOW)
+
+        @pl.when(seq > 0)
+        def _():
+            for copy in halo_copies(next_plane):
+                copy.wait_recv()
+            spread(halo_pairs[...].astype(f32), top, 1.0)
+            pool_span[pl.ds(WINDOW - HALO_ROWS, HALO_ROWS)] = halo_pool[...]
+
+        @pl.when(seq == 0)
+        def _():
+            for ref in (keys_low, keys_high, values_low, values_high):
+                ref[top] = jnp.zeros((WINDOW, ref.shape[1]), bf16)
+
+    half = blocks // 2
+
+    def mix_half(side):
+        @pl.loop(0, half)
+        def _(index):
+            block = side * half + (index + 1) % half
+
+            @pl.when(block == 0)
+            def _():
+                take_halo()
+
+            pool(block)
+            attend(block)
+
+    mix_half(1 - x)
+    last.share_taken()
+    last.pass_on(0, 1 - y)
+    last.done = 2
     last.taken_pair().wait_recv()
+    for event in range(2):
+        each(event, "first_rows")
+    mix_half(x)
+    for event in range(2):
+        each(event, "other_rows")
+
     total = len(last.events)
 
+    def all_sent(index, whole):
+        remote(
+            whole, whole, sum_send.at[index], sum_recv.at[0, 0], place.sibling()
+        ).wait_send()
+
     def early_sends():
-        for chunk in range(TOKEN_CHUNKS):
-            to_x(chunk).wait_send()
-            to_y(chunk).wait_send()
+        def tokens_sent(index):
+            remote(
+                tokens, tokens, send_sem.at[index], near_sem.at[0, 0], place.sibling()
+            ).wait_send()
+
+        tokens_sent(1)
+        tokens_sent(2)
 
         @pl.when(away)
         def _():
-            for chunk in range(TOKEN_CHUNKS):
-                to_sibling(chunk).wait_send()
+            tokens_sent(0)
 
         @pl.when(home)
         def _():
@@ -1024,12 +1034,14 @@
         last.sent_edges(last_gave)
         for event in range(total):
             first.sent(event)
+        if place.planes > 1:
+            first.shared(first_weights.at[pl.ds(0, (place.planes - 1) * depth)])
 
     for event, (step, slot) in enumerate(last.events):
         last.upto(event)
         if step > 0:
             last.complete(step, slot)
-        each(event, "first")
+            each(event, "first")
         if event > 0:
             each(event - 1, "second")
         if event > 2:
@@ -1038,13 +1050,25 @@
             early_sends()
         if event > 3:
             last.sent(event - 4)
-            each(event - 4, "sent")
     each(total - 1, "second")
     for event in range(max(0, total - 3), total):
         each(event, "third")
     for event in range(max(0, total - 4), total):
         last.sent(event)
-        each(event, "sent")
+    if place.planes > 1:
+        last.shared(last_weights.at[pl.ds(0, place.planes - 1)])
+    all_sent(0, from_x)
+
+    @pl.when(home)
+    def _():
+        all_sent(1, from_pair)
+
+    @pl.when(away)
+    def _():
+        all_sent(1, from_away)
+
+    for core in range(2):
+        all_sent(2 + core, from_last.at[:, pl.ds(0, from_x.shape[1])])
 
 
 def layer(tokens, w_pool_in, w_query, w_key_t, w_value_t, pool_map, w_out, *rows_in):
@@ -1098,18 +1122,19 @@
             pltpu.VMEM((1, GROUP), f32),
             pltpu.VMEM((8, LANES), f32),
             dma((12,)),
-            dma((4, 2, planes, 2)),
-            dma((4, 2, planes, 2)),
-            dma((7,)),
-            dma((7,)),
+            dma((3, 2, max(1, planes - 1), 2)),
+            dma((3, 2, max(1, planes - 1), 2)),
+            dma((8,)),
+            dma((8,)),
             dma((2, TOKEN_CHUNKS)),
             dma((2, TOKEN_CHUNKS)),
-            dma((3, TOKEN_CHUNKS)),
+            dma((3,)),
             dma((2, TOKEN_CHUNKS)),
             dma((2, 3)),
             dma((2, 2)),
-            dma((6, count)),
+            dma((4,)),
             dma((4, count)),
+            dma((2,)),
         ],
         compiler_params=pltpu.CompilerParams(
             collective_id=0, has_side_effects=True, vmem_limit_bytes=60 * 1024 * 1024

time: 175 us -> 173 us (0.989)
  Pallas kernels: 174 us -> 172 us
where the time goes in v4:
time: 173 us
  Pallas kernels  172 us (99%)
    pallas_call x1, Pallas kernels, layer(): pl.pallas_call(functools.partial(layer_kernel, count), out_shape=pltpu.VM...  172 us

profile of v4, /device:TPU:1, one launch (start us, length us, event | category | flops | bytes accessed | tf_op | source)
XLA Modules:
  0.0 173.3 jit_solution(7181690868831947207)
XLA Ops:
  0.0 172.0 %shard_map.118 = bf16[256,4096]{1,0:T(8,128)(2,1)S(1)} custom-call(bf16[1024,1024]{1,0:T(8,128)(2,1)} %tokens.1, bf16[512,512]{1,0:T(8,128)(2,1)} %w_pool_in.1, bf16[512,512]{1,0:T(8,128)(2,1)} %w_query.1, bf16[64,512]{1,0:T(8,128)(2,1)} %bitcast.9, bf16[64,512]{1,0:T(8,128)(2,1)} %bitcast.10, bf16[512,512]{1,0:T(8,128)(2,1)} %bitcast.8, ...), custom_call_target="tpu_custom_call" | custom-call | flops 18253611008 | bytes 4194304 | tf_op jit(solution)/shard_map/pallas_call | solution.py:1088
  172.0 1.3 copy.14

commit v5 on v4

--- a/solution.py
+++ b/solution.py
@@ -71,33 +71,50 @@
 
 
 class Chain:
-    def __init__(self, place, shard, own_first, sems):
+    def __init__(self, place, shard, own_first, sems, cuts=1):
         self.place, self.shard, self.own_first = place, shard, own_first
         self.up_send, self.up_recv, self.pair_recv, self.edge = sems
-        self.events = [(step, slot) for step in range(place.planes) for slot in range(2)]
+        self.cuts = cuts if place.planes > 2 else 1
+        self.events = [(step, slot, None) for step in range(place.planes) for slot in range(2)]
+        if self.cuts > 1:
+            step, slot, _ = self.events.pop()
+            self.events += [(step, slot, cut) for cut in range(cuts)]
         self.done, self.whole = 0, set()
 
-    def block(self, plane, slot, half):
+    def cuts_of(self, step, slot):
+        if self.cuts > 1 and step == self.place.planes - 1 and slot == 1:
+            return range(self.cuts)
+        return [None]
+
+    def block(self, plane, slot, half, cut=None):
         side = slot if not self.own_first else (self.place.y + slot) % 2
-        return self.shard(2 * plane + side, half)
-
-    def hop(self, way, step, slot):
-        held = self.block(self.place.source(way, step), slot, self.place.c)
+        if cut is None:
+            return self.shard(2 * plane + side, half)
+        return self.shard(2 * plane + side, half, cut)
+
+    def hop(self, way, step, slot, cut=None):
+        held = self.block(self.place.source(way, step), slot, self.place.c, cut)
         return remote(
             held,
             held,
-            self.up_send.at[way, step, slot],
-            self.up_recv.at[way, step, slot],
+            self.edge.at[8 + way] if cut == 1 else self.up_send.at[way, step, slot],
+            self.edge.at[10 + way] if cut == 1 else self.up_recv.at[way, step, slot],
             self.place.along_z(way),
         )
 
-    def pair(self, way, step, slot):
-        held = self.block(self.place.source(way, step), slot, self.place.c)
+    def hops(self, way, step, slot):
+        return [
+            self.hop(way, step, slot, cut)
+            for cut in (self.cuts_of(step + 1, slot) if step > 0 else [None])
+        ]
+
+    def pair(self, way, step, slot, cut=None):
+        held = self.block(self.place.source(way, step), slot, self.place.c, cut)
         return remote(
             held,
             held,
             self.edge.at[7],
-            self.pair_recv.at[way, step - 1, slot],
+            self.edge.at[12 + way] if cut == 1 else self.pair_recv.at[way, step - 1, slot],
             self.place.sibling(),
         )
 
@@ -129,7 +146,8 @@
 
             @pl.when(self.place.passes(way))
             def _(way=way):
-                self.hop(way, step, slot).start()
+                for copy in self.hops(way, step, slot):
+                    copy.start()
 
     def share_own(self):
         @pl.when(self.place.home)
@@ -156,7 +174,7 @@
         )
 
     def advance(self):
-        step, slot = self.events[self.done]
+        step, slot, cut = self.events[self.done]
         self.done += 1
         if step == 0:
             if self.own_first:
@@ -171,22 +189,23 @@
 
             @pl.when(self.place.has(way, step))
             def _(way=way):
-                self.hop(way, step - 1, slot).wait_recv()
-                self.pair(way, step, slot).start()
+                self.hop(way, step - 1, slot, cut).wait_recv()
+                self.pair(way, step, slot, cut).start()
                 if step + 1 < self.place.planes:
 
                     @pl.when(self.place.passes(way))
                     def _():
-                        self.hop(way, step, slot).start()
+                        for copy in self.hops(way, step, slot):
+                            copy.start()
 
     def upto(self, event):
         while self.done <= min(event, len(self.events) - 1):
             self.advance()
 
-    def complete(self, step, slot):
-        if (step, slot) in self.whole:
+    def complete(self, step, slot, cut=None):
+        if (step, slot, cut) in self.whole:
             return
-        self.whole.add((step, slot))
+        self.whole.add((step, slot, cut))
         if step == 0:
             if slot == 1:
                 self.taken_pair().wait_recv()
@@ -195,7 +214,7 @@
 
             @pl.when(self.place.has(way, step))
             def _(way=way):
-                self.pair(way, step, slot).wait_recv()
+                self.pair(way, step, slot, cut).wait_recv()
 
     def sent_edges(self, gave):
         @pl.when(self.place.home)
@@ -210,14 +229,15 @@
         self.taken_pair().wait_send()
 
     def sent(self, event):
-        step, slot = self.events[event]
+        step, slot, _ = self.events[event]
         place = self.place
         if step + 1 < place.planes:
             for way in range(2):
 
                 @pl.when(place.has(way, step) & place.passes(way))
                 def _(way=way):
-                    self.hop(way, step, slot).wait_send()
+                    for copy in self.hops(way, step, slot):
+                        copy.wait_send()
 
     def shared(self, whole):
         remote(
@@ -325,15 +345,25 @@
         size = depth // 2
         return first_weights.at[pl.ds(pl.multiple_of(owner * depth + half * size, size), size)]
 
-    def last_shard(owner, half):
+    def last_shard(owner, half, cut=None):
         if half is None:
             return last_weights.at[owner]
+        if cut is not None:
+            size = out_width // 2
+            return last_weights.at[owner, aligned(half, mix // 2), pl.ds((1 - cut) * size, size)]
         return last_weights.at[owner, aligned(half, mix // 2)]
 
     first = Chain(
         place, first_shard, True, [first_sems.at[i] for i in range(3)] + [first_edge]
     )
-    last = Chain(place, last_shard, False, [last_sems.at[i] for i in range(3)] + [last_edge])
+    halves = out_width % (2 * LANES) == 0
+    last = Chain(
+        place,
+        last_shard,
+        False,
+        [last_sems.at[i] for i in range(3)] + [last_edge],
+        2 if halves else 1,
+    )
 
     def local_copy(index, source, target):
         return pltpu.make_async_copy(source, target, local_sem.at[index])
@@ -569,9 +599,11 @@
                 def _(way=way):
                     block = aligned(place.source(way, step), 2 * depth)
 
-                    @pl.loop(chunks[0], chunks[1])
+                    size = tile * (2 if (chunks[0] | chunks[1]) % 2 == 0 else 1)
+
+                    @pl.loop(chunks[0] * tile // size, chunks[1] * tile // size)
                     def _(index):
-                        held = aligned(index, tile)
+                        held = aligned(index, size)
                         acc[held] += dot(normed[held, block], first_weights[block, :])
 
     class Progress:
@@ -772,7 +804,7 @@
         for pair, part in enumerate(parts):
             mixed[held, pl.ds(branch + pair * LANES, LANES)] = (part * scale).astype(bf16)
 
-    if out_width % (2 * LANES) == 0:
+    if halves:
         units_of = {0: [(1, 0), (2, out_width // 2)], 1: [(1, 0), (2, out_width // 2)]}
         unit_width = out_width // 2
     else:
@@ -783,9 +815,10 @@
 
     class Shard:
         def __init__(self, owner, event):
-            slot = last.events[event][1]
+            slot, self.cut = last.events[event][1:]
             self.owner, self.event = owner, event
-            self.units = units_of[slot]
+            self.units = units_of[slot] if self.cut is None else [units_of[slot][1 - self.cut]]
+            self.columns = (0, out_width) if self.cut is None else (self.units[0][1], unit_width)
 
         def lanes(self, start, size):
             return pl.ds(pl.multiple_of(self.owner * out_width + start, step_of), size)
@@ -794,7 +827,7 @@
             return self.lanes(start, unit_width)
 
         def packed(self):
-            return aligned(self.owner if len(self.units) == 2 else self.owner // 2, unit_width)
+            return aligned(self.owner if halves else self.owner // 2, unit_width)
 
         def copy(self, source, target, sent, landed, device):
             return remote(
@@ -828,12 +861,12 @@
             )
 
         def to_pair(self):
-            lanes = self.lanes(0, out_width)
-            return self.copy(
+            lanes = self.lanes(*self.columns)
+            return remote(
                 self.row_block(2 * x + 1 - c, lanes),
                 from_pair.at[:, lanes],
-                1,
-                1,
+                sum_send.at[1],
+                half_recv.at[2] if self.cut == 1 else sum_recv.at[1, self.owner],
                 place.sibling(),
             )
 
@@ -858,12 +891,13 @@
             )
 
         def terms(self, least, end):
-            lanes = self.lanes(0, out_width)
+            lanes = self.lanes(*self.columns)
 
             @pl.loop(least, end)
             def _(index):
                 held = aligned((2 * (1 - x) + index) % 4, out_rows)
-                normed[held, lanes] = dot(mixed[held, :], last_weights[self.owner]).astype(bf16)
+                value = dot(mixed[held, :], last_weights[self.owner, :, pl.ds(*self.columns)])
+                normed[held, lanes] = value.astype(bf16)
 
         def go_across(self, part):
             for scheme, start in self.units:
@@ -928,7 +962,7 @@
                 self.to_pair().start()
 
         def third(self):
-            lanes = self.lanes(0, out_width)
+            lanes = self.lanes(*self.columns)
             for scheme, start in self.units:
                 if scheme == 1:
                     self.away_final(start, 0).wait_recv()
@@ -950,7 +984,7 @@
                 ).astype(bf16)
 
     def each(event, stage):
-        step, slot = last.events[event]
+        step, slot, _ = last.events[event]
 
         @pl.loop(0, 1 if step == 0 else 2)
         def _(way):
@@ -1032,17 +1066,18 @@
 
         first.sent_edges(first_gave)
         last.sent_edges(last_gave)
-        for event in range(total):
+        for event in range(events):
             first.sent(event)
         if place.planes > 1:
             first.shared(first_weights.at[pl.ds(0, (place.planes - 1) * depth)])
 
-    for event, (step, slot) in enumerate(last.events):
+    for event, (step, slot, cut) in enumerate(last.events):
         last.upto(event)
         if step > 0:
-            last.complete(step, slot)
+            last.complete(step, slot, cut)
             each(event, "first")
-        if event > 0:
+        waits = False
+        if event > 0 and not waits:
             each(event - 1, "second")
         if event > 2:
             each(event - 3, "third")
@@ -1125,7 +1160,7 @@
             dma((3, 2, max(1, planes - 1), 2)),
             dma((3, 2, max(1, planes - 1), 2)),
             dma((8,)),
-            dma((8,)),
+            dma((14,)),
             dma((2, TOKEN_CHUNKS)),
             dma((2, TOKEN_CHUNKS)),
             dma((3,)),
@@ -1134,7 +1169,7 @@
             dma((2, 2)),
             dma((4,)),
             dma((4, count)),
-            dma((2,)),
+            dma((3,)),
         ],
         compiler_params=pltpu.CompilerParams(
             collective_id=0, has_side_effects=True, vmem_limit_bytes=60 * 1024 * 1024

time: 173 us -> 172 us (level)
  no operation moved by 1% of the time
where the time goes in v5:
time: 172 us
  Pallas kernels  171 us (99%)
    pallas_call x1, Pallas kernels, layer(): pl.pallas_call(functools.partial(layer_kernel, count), out_shape=pltpu.VM...  171 us

profile of v5, /device:TPU:1, one launch (start us, length us, event | category | flops | bytes accessed | tf_op | source)
XLA Modules:
  0.0 172.3 jit_solution(12148509137359352653)
XLA Ops:
  0.0 171.0 %shard_map.118 = bf16[256,4096]{1,0:T(8,128)(2,1)S(1)} custom-call(bf16[1024,1024]{1,0:T(8,128)(2,1)} %tokens.1, bf16[512,512]{1,0:T(8,128)(2,1)} %w_pool_in.1, bf16[512,512]{1,0:T(8,128)(2,1)} %w_query.1, bf16[64,512]{1,0:T(8,128)(2,1)} %bitcast.9, bf16[64,512]{1,0:T(8,128)(2,1)} %bitcast.10, bf16[512,512]{1,0:T(8,128)(2,1)} %bitcast.8, ...), custom_call_target="tpu_custom_call" | custom-call | flops 18253611008 | bytes 4194304 | tf_op jit(solution)/shard_map/pallas_call | solution.py:1123
  171.0 1.3 copy.14

commit v6 on v5

--- a/solution.py
+++ b/solution.py
@@ -893,9 +893,9 @@
         def terms(self, least, end):
             lanes = self.lanes(*self.columns)
 
-            @pl.loop(least, end)
+            @pl.loop(least // 2, end // 2)
             def _(index):
-                held = aligned((2 * (1 - x) + index) % 4, out_rows)
+                held = aligned((1 - x + index) % 2, 2 * out_rows)
                 value = dot(mixed[held, :], last_weights[self.owner, :, pl.ds(*self.columns)])
                 normed[held, lanes] = value.astype(bf16)
 

time: 172 us -> 172 us (level)
  no operation moved by 1% of the time
where the time goes in v6:
time: 172 us
  Pallas kernels  171 us (99%)
    pallas_call x1, Pallas kernels, layer(): pl.pallas_call(functools.partial(layer_kernel, count), out_shape=pltpu.VM...  171 us

profile of v6, /device:TPU:1, one launch (start us, length us, event | category | flops | bytes accessed | tf_op | source)
XLA Modules:
  0.0 172.0 jit_solution(13594565391481307384)
XLA Ops:
  0.0 170.6 %shard_map.118 = bf16[256,4096]{1,0:T(8,128)(2,1)S(1)} custom-call(bf16[1024,1024]{1,0:T(8,128)(2,1)} %tokens.1, bf16[512,512]{1,0:T(8,128)(2,1)} %w_pool_in.1, bf16[512,512]{1,0:T(8,128)(2,1)} %w_query.1, bf16[64,512]{1,0:T(8,128)(2,1)} %bitcast.9, bf16[64,512]{1,0:T(8,128)(2,1)} %bitcast.10, bf16[512,512]{1,0:T(8,128)(2,1)} %bitcast.8, ...), custom_call_target="tpu_custom_call" | custom-call | flops 18253611008 | bytes 4194304 | tf_op jit(solution)/shard_map/pallas_call | solution.py:1123
  170.6 1.3 copy.14
